TPU v7x, 128 devices: a whole 4x4x4 slice. The times are simulated.
128 devices in a mesh: sp: 32 (over z, y, core), tp: 4 (over x).
Axes of the slice: x: 4, y: 4, z: 4, core: 2. Of those that a mesh axis runs over, the one named last changes fastest.
Arguments:
- residual: bfloat16 [8192, 2048], P(('sp', 'tp')), may hold values from -6 to 6
- ssm_input: bfloat16 [8192, 2048], P('sp', 'tp'), may hold values from -6 to 6
- pole_real: float32 [128, 64], P('tp'), may hold values from -2 to 0
- pole_imaginary: float32 [128, 64], P('tp'), may hold values from 1 to 100
- step_log: float32 [128], P('tp'), may hold values from -8 to 0
- input_real: float32 [128, 64, 16], P('tp'), may hold values from -1 to 1
- entry_map_quadrature: float32 [128, 64, 16], P('tp'), may hold values from -1 to 1
- output_real: float32 [128, 16, 64], P('tp'), may hold values from -0.5 to 0.5
- output_imaginary: float32 [128, 16, 64], P('tp'), may hold values from -0.5 to 0.5
- added_log_decay: float32 [8192, 128], P('sp', 'tp'), may hold values from -2 to 0
- out_weight: bfloat16 [2048, 2048], P('tp'), may hold values from -0.125 to 0.125
- mix_gain: float32 [2048], replicated, may hold values from 0.1 to 1.9
- gate_weight: bfloat16 [2048, 5632], P('sp', 'tp'), may hold values from -0.125 to 0.125
- up_weight: bfloat16 [2048, 5632], P('sp', 'tp'), may hold values from -0.125 to 0.125
- down_weight: bfloat16 [2048, 5632], P('sp', 'tp'), may hold values from -0.078125 to 0.078125
- pre_gain: float32 [2048], replicated, may hold values from 0.1 to 1.9
- post_gain: float32 [2048], replicated, may hold values from 0.1 to 1.9
Outputs:
- merged: bfloat16 [8192, 2048], P(('sp', 'tp'))
All inputs are finite; a program needn't handle non-finite values.
Results may differ from a plain program's by a relative error of at most 0.017.
Values may be sent and summed in bfloat16 or wider, within the bound.
A program may use at most 128 MiB of HBM per device.

v0:
```python
import functools

import jax
import jax.numpy as jnp
from jax import lax
from jax.experimental import pallas as pl
from jax.experimental.pallas import tpu as pltpu
from jax.sharding import PartitionSpec as P

EPSILON = 1e-06
EXACT = lax.Precision.HIGHEST
MESH = pl.DeviceIdType.MESH
F32 = jnp.float32
BF16 = jnp.bfloat16
T = 256
G = 32
N = 64
C = 16
GN = G * N
SEGS = 8
STEPS = T // SEGS


def dot(a, b, **kw):
    return jnp.dot(a, b, preferred_element_type=F32, **kw)


def dot_nt(a, b):
    return lax.dot_general(a, b, (((1,), (1,)), ((), ())), preferred_element_type=F32)


def iota(shape, dim):
    return lax.broadcasted_iota(jnp.int32, shape, dim)


def one_hot(mask, dtype):
    return jnp.where(mask, 1.0, 0.0).astype(dtype)


def cmul(ar, ai, br, bi):
    return ar * br - ai * bi, ar * bi + ai * br


def split(v):
    hi = v.astype(BF16)
    return hi, (v - hi.astype(F32)).astype(BF16)


def expm1(x):
    p = 1.0 / 40320.0
    for k in (5040.0, 720.0, 120.0, 24.0, 6.0, 2.0, 1.0):
        p = p * x + 1.0 / k
    return jnp.where(x > -0.5, p * x, jnp.exp(x) - 1.0)


def step_rows(pr_ref, pi_ref, sl_ref):
    tile = one_hot(iota((N, GN), 1) % N == iota((N, GN), 0), F32)
    mine = iota((G, GN), 1) // N == iota((G, GN), 0)
    groups = one_hot(mine, F32)

    def row(ref):
        wide = dot(ref[...], tile, precision=EXACT)
        return jnp.sum(jnp.where(mine, wide, 0.0), axis=0, keepdims=True)

    pr, pi = row(pr_ref), row(pi_ref)
    sl = dot(jnp.broadcast_to(sl_ref[...], (8, G)), groups, precision=EXACT)[0:1]
    step = jnp.exp(sl)
    log_size = pr * step
    angle = pi * step
    cosine, sine = jnp.cos(angle), jnp.sin(angle)
    size = jnp.exp(log_size)
    half = jnp.sin(0.5 * angle)
    lift_r = expm1(log_size) * cosine - 2.0 * half * half
    lift_i = size * sine
    inv = 1.0 / (pr * pr + pi * pi)
    ratio_r = (lift_r * pr + lift_i * pi) * inv
    ratio_i = (lift_i * pr - lift_r * pi) * inv
    return size * cosine, size * sine, ratio_r, ratio_i, groups


def scan_pass(base, e_ref, dr_ref, di_ref, init, store):
    ends = []
    width = GN // 4
    for lc in range(4):
        sl = slice(lc * width, (lc + 1) * width)
        br = jnp.broadcast_to(base[0][:, sl], (SEGS, width))
        bi = jnp.broadcast_to(base[1][:, sl], (SEGS, width))

        def body(i, st):
            sr, si, pe = st
            rows = pl.ds(pl.multiple_of(i * SEGS, SEGS), SEGS)
            e = e_ref[rows, sl]
            ar, ai = br * e, bi * e
            nr = ar * sr - ai * si + dr_ref[rows, sl]
            ni = ar * si + ai * sr + di_ref[rows, sl]
            if store:
                dr_ref[rows, sl] = nr
                di_ref[rows, sl] = ni
                return nr, ni, pe
            return nr, ni, pe * e

        st = (init[0][:, sl], init[1][:, sl], jnp.ones((SEGS, width), F32))
        ends.append(lax.fori_loop(0, STEPS, body, st, unroll=4))
    return [jnp.concatenate([p[k] for p in ends], axis=1) for k in range(3)]


def put_row(ref, slot, part, row):
    for k in range(16):
        ref[slot, part * 16 + k : part * 16 + k + 1, :] = row[:, k * 128 : (k + 1) * 128]


def to_row(block):
    return jnp.concatenate([block[k : k + 1, :] for k in range(16)], axis=1)


def parts_of(ref, slot):
    block = ref[slot]
    return [block[16 * k : 16 * (k + 1), :] for k in range(4)]


def link(first, then):
    ar, ai, sr, si = first
    br, bi, tr, ti = then
    pr, pi = cmul(br, bi, ar, ai)
    ur, ui = cmul(br, bi, sr, si)
    return pr, pi, ur + tr, ui + ti


def choose(cond, a, b):
    return tuple(jnp.where(cond, x, y) for x, y in zip(a, b))


def front_kernel(
    u_ref, a_ref, pr_ref, pi_ref, sl_ref, bre_ref, bim_ref, cre_ref, cim_ref, wo_ref,
    out_ref,
    e_ref, dr_ref, di_ref, act_ref, ra_ref, rb_ref, sa, qa, sb, qb,
):
    sp = lax.axis_index("sp")
    q = sp % 8
    z = sp // 8
    peers_a = [z * 8 + (q + d) % 8 for d in range(1, 8)]
    peers_b = [((z + d) % 4) * 8 + q for d in range(1, 4)]
    barrier = pltpu.get_barrier_semaphore()
    for peer in peers_a + peers_b:
        pl.semaphore_signal(barrier, inc=1, device_id={"sp": peer}, device_id_type=MESH)

    base_r, base_i, ratio_r, ratio_i, groups = step_rows(pr_ref, pi_ref, sl_ref)
    perm = iota((T, T), 1) == (iota((T, T), 0) % SEGS) * STEPS + iota((T, T), 0) // SEGS
    e_small = dot(one_hot(perm, F32), jnp.exp(a_ref[...]), precision=EXACT)
    e_ref[...] = dot(e_small, groups, precision=EXACT)
    u = dot(one_hot(perm, BF16), u_ref[...]).astype(BF16)
    spread = one_hot(iota((C, 256), 1) % C == iota((C, 256), 0), BF16)
    own_b = iota((1024, 256), 0) // N == iota((1024, 256), 1) // C
    for h in range(2):
        gn = slice(h * 1024, (h + 1) * 1024)
        uh = u[:, h * 256 : (h + 1) * 256]
        raw = []
        for ref in (bre_ref, bim_ref):
            acc = None
            for piece in split(ref[gn, :]):
                wide = jnp.where(own_b, dot(piece, spread), 0.0).astype(BF16)
                term = dot_nt(uh, wide)
                acc = term if acc is None else acc + term
            raw.append(acc)
        rr, ri = ratio_r[:, gn], ratio_i[:, gn]
        dr_ref[:, gn] = rr * raw[0] - ri * raw[1]
        di_ref[:, gn] = rr * raw[1] + ri * raw[0]

    zero = jnp.zeros((SEGS, GN), F32)
    end_r, end_i, pe = scan_pass((base_r, base_i), e_ref, dr_ref, di_ref, (zero, zero), False)
    wr, wi = base_r, base_i
    for _ in range(5):
        wr, wi = cmul(wr, wi, wr, wi)
    seg_r, seg_i = wr * pe, wi * pe
    one_row = jnp.ones((1, GN), F32)
    no_row = jnp.zeros((1, GN), F32)
    total = (one_row, no_row, no_row, no_row)
    before = []
    for j in range(SEGS):
        before.append(total)
        total = link(total, (seg_r[j : j + 1], seg_i[j : j + 1], end_r[j : j + 1], end_i[j : j + 1]))
    for k in range(4):
        put_row(ra_ref, 0, k, total[k])

    pl.semaphore_wait(barrier, 10)
    copies = []
    for d in range(1, 8):
        copies.append(pltpu.make_async_remote_copy(
            ra_ref.at[0], ra_ref.at[d], sa.at[d], qa.at[d],
            device_id={"sp": peers_a[d - 1]}, device_id_type=MESH))
        copies[-1].start()
    for copy in copies:
        copy.wait()
    unit = jnp.ones((16, 128), F32)
    null = jnp.zeros((16, 128), F32)
    run = (unit, null, null, null)
    pre_a = run
    for k in range(8):
        pre_a = choose(q == k, run, pre_a)
        run = link(run, parts_of(ra_ref, (q - k + 8) % 8))
    for k in range(4):
        rb_ref[0, 16 * k : 16 * (k + 1), :] = run[k]
    copies = []
    for d in range(1, 4):
        copies.append(pltpu.make_async_remote_copy(
            rb_ref.at[0], rb_ref.at[d], sb.at[d], qb.at[d],
            device_id={"sp": peers_b[d - 1]}, device_id_type=MESH))
        copies[-1].start()
    for copy in copies:
        copy.wait()
    run = (unit, null, null, null)
    pre_b = run
    for k in range(4):
        pre_b = choose(z == k, run, pre_b)
        run = link(run, parts_of(rb_ref, (z - k + 4) % 4))
    carry = link(pre_b, pre_a)
    cr, ci = to_row(carry[2]), to_row(carry[3])
    starts = []
    for k in range(SEGS):
        pr, pi, sr, si = before[k]
        tr, ti = cmul(pr, pi, cr, ci)
        starts.append((tr + sr, ti + si))
    init = [jnp.concatenate([s[k] for s in starts], axis=0) for k in range(2)]
    scan_pass((base_r, base_i), e_ref, dr_ref, di_ref, init, True)

    lay = one_hot(iota((N, 1024), 1) % N == iota((N, 1024), 0), BF16)
    own_c = iota((256, 1024), 0) // C == iota((256, 1024), 1) // N
    for h in range(2):
        gn = slice(h * 1024, (h + 1) * 1024)
        ch = slice(h * 256, (h + 1) * 256)
        y = None
        for s_ref, c_ref, sign in ((dr_ref, cre_ref, 1.0), (di_ref, cim_ref, -1.0)):
            s_hi, s_lo = split(s_ref[:, gn])
            c_hi, c_lo = (
                jnp.where(own_c, dot(piece, lay), 0.0).astype(BF16)
                for piece in split(sign * c_ref[ch, :])
            )
            term = dot_nt(s_hi, c_hi) + dot_nt(s_lo, c_hi) + dot_nt(s_hi, c_lo)
            y = term if y is None else y + term
        act_ref[:, ch] = jax.nn.gelu(y).astype(BF16)
    back = iota((T, T), 0) == (iota((T, T), 1) % SEGS) * STEPS + iota((T, T), 1) // SEGS
    act = dot(one_hot(back, BF16), act_ref[...]).astype(BF16)
    out_ref[...] = dot(act, wo_ref[...]).astype(BF16)


def front(u, a, pr, pi, sl, bre, bim, cre, cim, wo):
    vmem = pl.BlockSpec(memory_space=pltpu.VMEM)
    return pl.pallas_call(
        front_kernel,
        out_shape=jax.ShapeDtypeStruct((T, wo.shape[1]), BF16),
        in_specs=[vmem] * 10,
        out_specs=vmem,
        scratch_shapes=[
            pltpu.VMEM((T, GN), F32),
            pltpu.VMEM((T, GN), F32),
            pltpu.VMEM((T, GN), F32),
            pltpu.VMEM((T, 512), BF16),
            pltpu.VMEM((8, 64, 128), F32),
            pltpu.VMEM((4, 64, 128), F32),
            pltpu.SemaphoreType.DMA((8,)),
            pltpu.SemaphoreType.DMA((8,)),
            pltpu.SemaphoreType.DMA((4,)),
            pltpu.SemaphoreType.DMA((4,)),
        ],
        compiler_params=pltpu.CompilerParams(
            collective_id=0, has_side_effects=True, vmem_limit_bytes=56 * 1024 * 1024
        ),
        name="front",
    )(
        u, a, pr, pi, sl.reshape(1, G), bre.reshape(GN, C), bim.reshape(GN, C),
        cre.reshape(512, N), cim.reshape(512, N), wo,
    )


def from_everyone(shard, axis):
    copies = jnp.broadcast_to(shard, (lax.axis_size(axis), *shard.shape))
    return lax.all_to_all(copies, axis, split_axis=0, concat_axis=0, tiled=True)


def summed_on_arrival(shard, axis):
    count = lax.axis_size(axis)
    blocks = shard.reshape(count, -1, shard.shape[1])
    arrived = lax.all_to_all(blocks, axis, split_axis=0, concat_axis=0, tiled=True)
    return arrived.astype(F32).sum(axis=0)


def rms_scale(values, gain):
    return values * lax.rsqrt(jnp.mean(values * values, axis=-1, keepdims=True) + EPSILON) * gain


def round_half(values):
    return lax.optimization_barrier(values.astype(BF16))


def shards(
    residual, ssm_input, pole_real, pole_imaginary, step_log, input_real, entry_map_quadrature,
    output_real, output_imaginary, added_log_decay, out_weight, mix_gain, gate_weight, up_weight,
    down_weight, pre_gain, post_gain,
):
    partial = front(
        ssm_input, added_log_decay, pole_real, pole_imaginary, step_log, input_real,
        entry_map_quadrature, output_real, output_imaginary, out_weight,
    )
    mixed_own = summed_on_arrival(partial, "tp")
    middle = round_half(residual.astype(F32) + rms_scale(mixed_own, mix_gain))
    normed_own = rms_scale(middle.astype(F32), pre_gain).astype(BF16)
    mixer_input = from_everyone(normed_own, "tp").reshape(T, -1)
    both = jnp.concatenate((gate_weight, up_weight, down_weight), axis=1)
    whole = lax.all_gather(both, "sp", axis=0, tiled=True)
    f = gate_weight.shape[1]
    gate_full, up_full, down_full = whole[:, :f], whole[:, f : 2 * f], whole[:, 2 * f :]
    gate_act = jnp.dot(mixer_input, gate_full, preferred_element_type=F32)
    up_act = jnp.dot(mixer_input, up_full, preferred_element_type=F32)
    hidden = (jax.nn.silu(gate_act) * up_act).astype(BF16)
    mixer_own = summed_on_arrival(dot_nt(hidden, down_full).astype(BF16), "tp")
    merged = middle.astype(F32) + 0.5 * rms_scale(mixer_own, post_gain)
    return merged.astype(BF16)


def solution(mesh):
    return jax.shard_map(
        shards,
        mesh=mesh,
        in_specs=(
            P(("sp", "tp"), None), P("sp", "tp"), P("tp", None), P("tp", None), P("tp"),
            P("tp", None, None), P("tp", None, None), P("tp", None, None), P("tp", None, None),
            P("sp", "tp"), P("tp", None), P(), P("sp", "tp"), P("sp", "tp"), P("sp", "tp"),
            P(), P(),
        ),
        out_specs=P(("sp", "tp"), None),
        check_vma=False,
    )
```

profile of v0, /device:TPU:1, one launch (start us, length us, event | category | flops | bytes accessed | tf_op | source)
XLA Modules:
  0.0 128.9 jit_solution(15917582712693834478)
XLA Ops:
  6.5 0.0 copy-start
  6.5 0.0 all-gather.2.cloned.1.call-start
  6.5 2.0 %pad_maximum_fusion = bf16[64,4224]{1,0:T(8,128)(2,1)} fusion(bf16[64,1408]{1,0:T(8,128)(2,1)} %param.31, bf16[64,1408]{1,0:T(8,128)(2,1)} %param.30, bf16[64,1408]{1,0:T(8,128)(2,1)} %param.29), kind=kLoop, calls=%fused_computation.20 | loop fusion | flops 1622016 | bytes 1081344 | tf_op jit(solution)/shard_map/concatenate | solution.py:308
  8.5 0.0 all-gather.2.cloned.1.call-update
  8.6 1.5 %copy.20.a_ref = f32[256,32]{1,0:T(8,128)} copy(f32[256,32]{0,1:T(8,128)} %param.26) | data formatting | bytes 65536 | tf_op args[9]
  10.1 2.3 %copy.18 = f32[32,64,16]{2,1,0:T(8,128)} copy(f32[32,64,16]{1,2,0:T(8,128)} %param.22) | data formatting | bytes 262144 | tf_op args[5]
  12.4 0.0 copy-done
  12.4 1.3 %copy.19 = f32[32,64,16]{2,1,0:T(8,128)} copy(f32[32,64,16]{1,2,0:T(8,128)S(1)} %copy-done) | data formatting | bytes 262144 | tf_op args[6]
  13.7 34.5 %front.1 = bf16[256,2048]{1,0:T(8,128)(2,1)} custom-call(bf16[256,512]{1,0:T(8,128)(2,1)} %u_ref.1, f32[256,32]{1,0:T(8,128)} %copy.20.a_ref, f32[32,64]{1,0:T(8,128)} %pr_ref.1, f32[32,64]{1,0:T(8,128)} %pi_ref.1, f32[1,32]{1,0:T(1,128)} %bitcast.18, f32[2048,16]{1,0:T(8,128)} %bitcast.10, f32[2048,16]{1,0:T(8,128)} %bitcast.11, f32[512,64]{1,0:T(8,128)} %bitcast.16, ...), custom_call_target="tpu_custom_call" | custom-call | tf_op jit(solution)/shard_map/front/pallas_call | solution.py:248
  48.2 0.0 copy-start.1
  48.2 0.0 copy-start.2
  48.2 19.0 %all_to_all.15 = bf16[4,64,2048]{2,1,0:T(8,128)(2,1)S(1)} all-to-all(bf16[4,64,2048]{2,1,0:T(8,128)(2,1)} %bitcast.12), channel_id=1, replica_groups=mesh['sp'=32,'tp'=4] {'tp'}, dimensions={0} | all-to-all | bytes 2097152 | tf_op jit(solution)/shard_map/all_to_all | solution.py:283
  67.2 0.0 copy-start.3
  67.2 0.2 convert_reduce_fusion.1
  67.4 0.1 multiply_reduce_fusion.1
  67.5 0.0 copy-done.1
  67.5 0.0 copy-done.2
  67.5 0.1 add_convert_fusion
  67.7 0.2 fusion.23
  67.9 0.1 copy-done.3
  67.9 0.1 fusion.25
  68.0 0.1 broadcast_in_dim.2
  68.2 16.4 %all_to_all.16 = bf16[4,64,2048]{2,1,0:T(8,128)(2,1)S(1)} all-to-all(bf16[4,64,2048]{2,1,0:T(8,128)(2,1)S(1)} %broadcast_in_dim.2), channel_id=1, replica_groups=mesh['sp'=32,'tp'=4] {'tp'}, dimensions={0} | all-to-all | bytes 2097152 | tf_op jit(solution)/shard_map/all_to_all | solution.py:277
  84.6 4.1 %all-gather.2.cloned.1.call-done = bf16[2048,4224]{1,0:T(8,128)(2,1)} async-done(((bf16[64,4224]{1,0:T(8,128)(2,1)}), bf16[2048,4224]{1,0:T(8,128)(2,1)}) %all-gather.2.cloned.1.call-update) | async-done | bytes 17301520 | tf_op jit(solution)/shard_map/all_gather | solution.py:309
  88.7 5.6 %fusion.4 = f32[256,1408]{1,0:T(8,128)} fusion(bf16[256,2048]{1,0:T(8,128)(2,1)S(1)} %bitcast.13, bf16[2048,4224]{1,0:T(8,128)(2,1)} %all-gather.2.cloned.1.call-done), kind=kOutput, calls=%fused_computation.4 | convolution fusion | flops 1476395008 | bytes 8257536 | tf_op jit(solution)/shard_map/dot_general | solution.py:312
  94.2 8.2 %fusion.12 = bf16[256,2048]{1,0:T(8,128)(2,1)S(1)} fusion(bf16[2048,4224]{1,0:T(8,128)(2,1)} %all-gather.2.cloned.1.call-done, bf16[256,2048]{1,0:T(8,128)(2,1)S(1)} %bitcast.14, f32[256,1408]{1,0:T(8,128)} %fusion.4), kind=kOutput, calls=%fused_computation.8 | convolution fusion | flops 2955476992 | bytes 15073280 | tf_op jit(solution)/shard_map/dot_general | solution.py:29
  102.4 0.0 copy-start.4
  102.4 18.4 %all_to_all.17 = bf16[4,64,2048]{2,1,0:T(8,128)(2,1)S(1)} all-to-all(bf16[4,64,2048]{2,1,0:T(8,128)(2,1)S(1)} %bitcast.15), channel_id=1, replica_groups=mesh['sp'=32,'tp'=4] {'tp'}, dimensions={0} | all-to-all | bytes 2097152 | tf_op jit(solution)/shard_map/all_to_all | solution.py:283
  120.8 0.2 convert_reduce_fusion
  121.0 0.1 multiply_reduce_fusion
  121.2 0.0 copy-done.4
  121.2 0.9 fusion.26
  (3 shorter events, 0.0 us)
Async XLA Ops:
  6.5 5.8 %copy-start = (f32[32,64,16]{1,2,0:T(8,128)S(1)}, f32[32,64,16]{1,2,0:T(8,128)}, u32[]{:S(2)}) copy-start(f32[32,64,16]{1,2,0:T(8,128)} %param.23) | copy-start | bytes 393220
  6.5 82.1 %all-gather.2.cloned.1.call-start = ((), (), s32[]{:S(2)}) async-start(), calls=%async_computation.3 | async-start | bytes 17842176 | tf_op jit(solution)/shard_map/all_gather | solution.py:309
  48.2 19.4 %copy-start.1 = (bf16[64,2048]{1,0:T(8,128)(2,1)S(1)}, bf16[64,2048]{1,0:T(8,128)(2,1)}, u32[]{:S(2)}) copy-start(bf16[64,2048]{1,0:T(8,128)(2,1)} %param.17) | copy-start | bytes 786436
  48.2 19.4 %copy-start.2 = (f32[2048]{0:T(1024)S(1)}, f32[2048]{0:T(1024)}, u32[]{:S(2)}) copy-start(f32[2048]{0:T(1024)} %param.28) | copy-start | bytes 24580
  67.2 0.7 copy-start.3
  102.4 18.7 %copy-start.4 = (f32[2048]{0:T(1024)S(1)}, f32[2048]{0:T(1024)}, u32[]{:S(2)}) copy-start(f32[2048]{0:T(1024)} %param.33) | copy-start | bytes 24580
Sparse Core Ops, SparseCore 0:
  9.6 79.0 all-gather.1
where the time goes:
time: 129 us
  blocking collectives  53.9 us (42%)
  Pallas kernels  34.5 us (27%)
  matrix products  13.7 us (11%)
  between operations  13.5 us (10%)
  local copies, waits for them, and re-layouts  5.31 us (4%)
  waiting for transfers between devices  4.1 us (3%)
  other arithmetic  3.92 us (3%)
    all_to_all x2, blocking collectives, summed_on_arrival(): lax.all_to_all(blocks, axis, split_axis=0, concat_axis=0, tiled=True)  37.4 us
    pallas_call x1, Pallas kernels, front(): pl.pallas_call(front_kernel, out_shape=jax.ShapeDtypeStruct((T, wo.shape[...  34.5 us
    all_to_all x1, blocking collectives, from_everyone(): return lax.all_to_all(copies, axis, split_axis=0, concat_axis=0, tiled=True)  16.4 us
    dot_general x1, matrix products, dot_nt(): lax.dot_general(a, b, (((1,), (1,)), ((), ())), preferred_element_type=F32)  8.19 us
    dot_general x1, matrix products, shards(): gate_act = jnp.dot(mixer_input, gate_full, preferred_element_type=F32)  5.55 us
    unnamed x13, local copies, waits for them, and re-layouts  5.2 us
    all_gather x1, waiting for transfers between devices, shards(): whole = lax.all_gather(both, 'sp', axis=0, tiled=True)  4.09 us
  transfers between devices with their start and end apart: 1, of which 1 were waited for; matrix products, arithmetic and copies ran while one was open for 5% of the time, Pallas kernels for 27%

commit v1 on v0

--- a/solution.py
+++ b/solution.py
@@ -19,6 +19,11 @@
 GN = G * N
 SEGS = 8
 STEPS = T // SEGS
+D = 2048
+F = 1408
+ROWS = 64
+HALF = D // 2
+TILES = F // 128
 
 
 def dot(a, b, **kw):
@@ -130,38 +135,235 @@
     return tuple(jnp.where(cond, x, y) for x, y in zip(a, b))
 
 
-def front_kernel(
-    u_ref, a_ref, pr_ref, pi_ref, sl_ref, bre_ref, bim_ref, cre_ref, cim_ref, wo_ref,
+def rms_scale(values, gain):
+    return values * lax.rsqrt(jnp.mean(values * values, axis=-1, keepdims=True) + EPSILON) * gain
+
+
+class Gather:
+    def __init__(self, refs, send, recv, sp):
+        self.refs, self.send_sem, self.recv_sem = refs, send, recv
+        core, y, z = sp % 2, (sp // 2) % 4, sp // 8
+        self.core = core
+        self.fm, self.sm = 1 + 3 * core, 4 - 3 * core
+        f = y + core * (z - y)
+        s = z + core * (y - z)
+        self.fk = [f, (f + 3) % 4, (f + 1) % 4, (f + 2) % 4]
+        self.sk = [s, (s + 3) % 4, (s + 1) % 4, (s + 2) % 4]
+        self.f_next, self.f_prev = self.place(2, 0), self.place(1, 0)
+        self.s_next, self.s_prev = self.place(0, 2), self.place(0, 1)
+        self.partner = sp + 1 - 2 * core
+        self.started = []
+
+    def place(self, k, m):
+        return 2 * (self.fk[k] * self.fm + self.sk[m] * self.sm) + self.core
+
+    def block(self, p, k, m, half=None):
+        start = self.place(k, m) * ROWS
+        return self.rows(p, start, half)
+
+    def rows(self, p, start, half):
+        if half is None:
+            return self.refs[p].at[pl.ds(pl.multiple_of(start, ROWS), ROWS)]
+        return self.refs[p].at[pl.ds(pl.multiple_of(start + half * 32, 32), 32)]
+
+    def copy(self, p, slot, ref, dev):
+        return pltpu.make_async_remote_copy(
+            ref, ref, self.send_sem.at[p, slot], self.recv_sem.at[p, slot],
+            device_id={"sp": dev}, device_id_type=MESH)
+
+    def send(self, p, slot, ref, dev):
+        copy = self.copy(p, slot, ref, dev)
+        copy.start()
+        self.started.append(copy)
+
+    def arrive(self, p, slot, ref):
+        self.copy(p, slot, ref, self.partner).wait_recv()
+
+    def hand(self, p, k, m):
+        self.send(p, 20 + 4 * k + m, self.block(p, k, m), self.partner)
+
+    def along_s(self, p, k):
+        ref = self.block(p, k, 0)
+        self.send(p, 4 + 4 * k, ref, self.s_next)
+        self.send(p, 5 + 4 * k, ref, self.s_prev)
+
+    def onward(self, p, k):
+        self.arrive(p, 4 + 4 * k, self.block(p, k, 1))
+        self.arrive(p, 5 + 4 * k, self.block(p, k, 2))
+        self.send(p, 6 + 4 * k, self.block(p, k, 1, 0), self.s_next)
+        self.send(p, 7 + 4 * k, self.block(p, k, 2, 1), self.s_prev)
+        self.hand(p, k, 1)
+        self.hand(p, k, 2)
+
+    def stage0(self, p):
+        own = self.block(p, 0, 0)
+        self.send(p, 0, own, self.f_next)
+        self.send(p, 1, own, self.f_prev)
+        self.along_s(p, 0)
+        self.hand(p, 0, 0)
+
+    def stage1(self, p):
+        self.arrive(p, 0, self.block(p, 1, 0))
+        self.arrive(p, 1, self.block(p, 2, 0))
+        self.send(p, 2, self.block(p, 1, 0, 0), self.f_next)
+        self.send(p, 3, self.block(p, 2, 0, 1), self.f_prev)
+        self.along_s(p, 1)
+        self.hand(p, 1, 0)
+        self.onward(p, 0)
+        self.along_s(p, 2)
+        self.hand(p, 2, 0)
+
+    def stage2(self, p):
+        self.arrive(p, 2, self.block(p, 3, 0, 0))
+        self.arrive(p, 3, self.block(p, 3, 0, 1))
+        self.along_s(p, 3)
+        self.hand(p, 3, 0)
+        self.onward(p, 1)
+
+    def stage3(self, p):
+        self.onward(p, 2)
+        self.onward(p, 3)
+
+    def stage4(self, p):
+        for k in range(4):
+            self.arrive(p, 6 + 4 * k, self.block(p, k, 3, 0))
+            self.arrive(p, 7 + 4 * k, self.block(p, k, 3, 1))
+            self.hand(p, k, 3)
+
+    def stage5(self, p):
+        for k in range(4):
+            for m in range(4):
+                chip = 2 * (self.sk[k] * self.sm + self.fk[m] * self.fm)
+                ref = self.rows(p, (chip + 1 - self.core) * ROWS, None)
+                self.arrive(p, 20 + 4 * k + m, ref)
+
+
+class Across:
+    def __init__(self, x, send, recv):
+        self.x, self.send_sem, self.recv_sem = x, send, recv
+        self.next, self.prev, self.far = (x + 1) % 4, (x + 3) % 4, (x + 2) % 4
+        self.started = []
+
+    def copy(self, phase, slot, src, dst, dev):
+        return pltpu.make_async_remote_copy(
+            src, dst, self.send_sem.at[phase, slot], self.recv_sem.at[phase, slot],
+            device_id={"tp": dev}, device_id_type=MESH)
+
+    def send(self, phase, slot, src, dst, dev):
+        copy = self.copy(phase, slot, src, dst, dev)
+        copy.start()
+        self.started.append(copy)
+
+    def arrive(self, phase, slot, ref):
+        self.copy(phase, slot, ref, ref, self.next).wait_recv()
+
+    def rows(self, x, half=None):
+        if half is None:
+            return pl.ds(pl.multiple_of(x * ROWS, ROWS), ROWS)
+        return pl.ds(pl.multiple_of(x * ROWS + half * 32, 32), 32)
+
+    def first(self, phase, part, relay, landed):
+        self.send(phase, 0, part.at[0, self.rows(self.far)], relay.at[phase, 0], self.next)
+        self.send(phase, 3, part.at[0, self.rows(self.prev)], landed.at[phase, 1, 0], self.prev)
+
+    def second(self, phase, part, relay, landed):
+        self.send(phase, 1, part.at[1, self.rows(self.far)], relay.at[phase, 1], self.prev)
+        self.send(phase, 2, part.at[1, self.rows(self.next)], landed.at[phase, 0, 1], self.next)
+
+    def pass_on(self, phase, part, relay, landed):
+        for side, dev in ((0, self.next), (1, self.prev)):
+            self.arrive(phase, side, relay.at[phase, side])
+            total = relay[phase, side].astype(F32) + part[side, self.rows(dev)].astype(F32)
+            relay[phase, side] = total.astype(BF16)
+            self.send(phase, 4 + side, relay.at[phase, side], landed.at[phase, side, side], dev)
+
+    def total(self, phase, part, landed):
+        for slot, side, half in ((2, 0, 1), (3, 1, 0), (4, 0, 0), (5, 1, 1)):
+            self.arrive(phase, slot, landed.at[phase, side, half])
+        halves = [
+            part[h, self.rows(self.x)].astype(F32)
+            + landed[phase, 0, h].astype(F32)
+            + landed[phase, 1, h].astype(F32)
+            for h in range(2)
+        ]
+        return jnp.concatenate(halves, axis=1)
+
+    def share(self, ref):
+        own = ref.at[self.rows(self.x)]
+        self.send(2, 0, own, own, self.next)
+        self.send(2, 1, own, own, self.prev)
+
+    def share_on(self, ref):
+        self.arrive(2, 0, ref.at[self.rows(self.prev)])
+        self.arrive(2, 1, ref.at[self.rows(self.next)])
+        top = ref.at[self.rows(self.prev, 0)]
+        bottom = ref.at[self.rows(self.next, 1)]
+        self.send(2, 2, top, top, self.next)
+        self.send(2, 3, bottom, bottom, self.prev)
+
+    def shared(self, ref):
+        self.arrive(2, 2, ref.at[self.rows(self.far, 0)])
+        self.arrive(2, 3, ref.at[self.rows(self.far, 1)])
+
+
+def layer_kernel(
+    u_ref, a_ref, pr_ref, pi_ref, sl_ref, bre_ref, bim_ref, cre_ref, cim_ref,
+    mix_gain_ref, pre_gain_ref, post_gain_ref, wo_hbm, res_hbm, gate_hbm, up_hbm, down_hbm,
     out_ref,
-    e_ref, dr_ref, di_ref, act_ref, ra_ref, rb_ref, sa, qa, sb, qb,
+    e_ref, dr_ref, di_ref, act_ref, ra_ref, rb_ref, wo_ref, res_ref, gu_ref, dn_ref,
+    part_ref, relay_ref, landed_ref, rows_ref, hid_ref,
+    sa, qa, sb, qb, ws, wq, xs, xq, ls,
 ):
     sp = lax.axis_index("sp")
+    tp = lax.axis_index("tp")
     q = sp % 8
     z = sp // 8
     peers_a = [z * 8 + (q + d) % 8 for d in range(1, 8)]
     peers_b = [((z + d) % 4) * 8 + q for d in range(1, 4)]
+    weights = Gather((gu_ref, dn_ref), ws, wq, sp)
+    across = Across(tp, xs, xq)
+    own = pl.ds(pl.multiple_of(sp * ROWS, ROWS), ROWS)
+    loads = []
+    for j in range(TILES):
+        for side, hbm in ((0, gate_hbm), (1, up_hbm)):
+            loads.append(pltpu.make_async_copy(
+                hbm.at[:, pl.ds(j * 128, 128)],
+                gu_ref.at[own, pl.ds((2 * j + side) * 128, 128)], ls.at[2 * j + side]))
+    loads.append(pltpu.make_async_copy(down_hbm, dn_ref.at[own], ls.at[2 * TILES]))
+    loads.append(pltpu.make_async_copy(wo_hbm, wo_ref, ls.at[2 * TILES + 1]))
+    loads.append(pltpu.make_async_copy(res_hbm, res_ref, ls.at[2 * TILES + 2]))
+    for load in loads:
+        load.start()
     barrier = pltpu.get_barrier_semaphore()
     for peer in peers_a + peers_b:
         pl.semaphore_signal(barrier, inc=1, device_id={"sp": peer}, device_id_type=MESH)
+    for peer in (across.next, across.prev):
+        pl.semaphore_signal(barrier, inc=1, device_id={"tp": peer}, device_id_type=MESH)
+    for load in loads[: 2 * TILES]:
+        load.wait()
+    pl.semaphore_wait(barrier, 12)
+    weights.stage0(0)
 
     base_r, base_i, ratio_r, ratio_i, groups = step_rows(pr_ref, pi_ref, sl_ref)
-    perm = iota((T, T), 1) == (iota((T, T), 0) % SEGS) * STEPS + iota((T, T), 0) // SEGS
-    e_small = dot(one_hot(perm, F32), jnp.exp(a_ref[...]), precision=EXACT)
-    e_ref[...] = dot(e_small, groups, precision=EXACT)
-    u = dot(one_hot(perm, BF16), u_ref[...]).astype(BF16)
-    spread = one_hot(iota((C, 256), 1) % C == iota((C, 256), 0), BF16)
-    own_b = iota((1024, 256), 0) // N == iota((1024, 256), 1) // C
+    perm = iota((T, T), 0) == (iota((T, T), 1) % SEGS) * STEPS + iota((T, T), 1) // SEGS
+    e_small = dot(jnp.exp(a_ref[...]), one_hot(perm, F32), precision=EXACT)
+    e_ref[...] = lax.dot_general(
+        e_small, groups, (((0,), (0,)), ((), ())), precision=EXACT, preferred_element_type=F32)
+    order = iota((T, T), 1) == (iota((T, T), 0) % SEGS) * STEPS + iota((T, T), 0) // SEGS
+    u = dot(one_hot(order, BF16), u_ref[...]).astype(BF16)
+    lay = one_hot(iota((N, 1024), 1) % N == iota((N, 1024), 0), BF16)
+    inside = iota((256, 1024), 0) // C == iota((256, 1024), 1) // N
+
+    def spread(v):
+        return [jnp.where(inside, dot(piece, lay), 0.0).astype(BF16) for piece in split(v)]
+
     for h in range(2):
         gn = slice(h * 1024, (h + 1) * 1024)
-        uh = u[:, h * 256 : (h + 1) * 256]
+        ch = slice(h * 256, (h + 1) * 256)
         raw = []
         for ref in (bre_ref, bim_ref):
-            acc = None
-            for piece in split(ref[gn, :]):
-                wide = jnp.where(own_b, dot(piece, spread), 0.0).astype(BF16)
-                term = dot_nt(uh, wide)
-                acc = term if acc is None else acc + term
-            raw.append(acc)
+            hi, lo = spread(ref[ch, :])
+            raw.append(dot(u[:, ch], hi) + dot(u[:, ch], lo))
         rr, ri = ratio_r[:, gn], ratio_i[:, gn]
         dr_ref[:, gn] = rr * raw[0] - ri * raw[1]
         di_ref[:, gn] = rr * raw[1] + ri * raw[0]
@@ -182,7 +384,6 @@
     for k in range(4):
         put_row(ra_ref, 0, k, total[k])
 
-    pl.semaphore_wait(barrier, 10)
     copies = []
     for d in range(1, 8):
         copies.append(pltpu.make_async_remote_copy(
@@ -206,6 +407,9 @@
             rb_ref.at[0], rb_ref.at[d], sb.at[d], qb.at[d],
             device_id={"sp": peers_b[d - 1]}, device_id_type=MESH))
         copies[-1].start()
+    weights.stage1(0)
+    loads[2 * TILES].wait()
+    weights.stage0(1)
     for copy in copies:
         copy.wait()
     run = (unit, null, null, null)
@@ -223,32 +427,77 @@
     init = [jnp.concatenate([s[k] for s in starts], axis=0) for k in range(2)]
     scan_pass((base_r, base_i), e_ref, dr_ref, di_ref, init, True)
 
-    lay = one_hot(iota((N, 1024), 1) % N == iota((N, 1024), 0), BF16)
-    own_c = iota((256, 1024), 0) // C == iota((256, 1024), 1) // N
     for h in range(2):
         gn = slice(h * 1024, (h + 1) * 1024)
         ch = slice(h * 256, (h + 1) * 256)
         y = None
         for s_ref, c_ref, sign in ((dr_ref, cre_ref, 1.0), (di_ref, cim_ref, -1.0)):
             s_hi, s_lo = split(s_ref[:, gn])
-            c_hi, c_lo = (
-                jnp.where(own_c, dot(piece, lay), 0.0).astype(BF16)
-                for piece in split(sign * c_ref[ch, :])
-            )
+            c_hi, c_lo = spread(sign * c_ref[ch, :])
             term = dot_nt(s_hi, c_hi) + dot_nt(s_lo, c_hi) + dot_nt(s_hi, c_lo)
             y = term if y is None else y + term
         act_ref[:, ch] = jax.nn.gelu(y).astype(BF16)
-    back = iota((T, T), 0) == (iota((T, T), 1) % SEGS) * STEPS + iota((T, T), 1) // SEGS
-    act = dot(one_hot(back, BF16), act_ref[...]).astype(BF16)
-    out_ref[...] = dot(act, wo_ref[...]).astype(BF16)
-
-
-def front(u, a, pr, pi, sl, bre, bim, cre, cim, wo):
+    act = dot(one_hot(perm, BF16), act_ref[...]).astype(BF16)
+    loads[2 * TILES + 1].wait()
+    part_ref[0, 0] = dot(act, wo_ref[:, :HALF]).astype(BF16)
+    across.first(0, part_ref.at[0], relay_ref, landed_ref)
+    part_ref[0, 1] = dot(act, wo_ref[:, HALF:]).astype(BF16)
+    across.second(0, part_ref.at[0], relay_ref, landed_ref)
+    weights.stage2(0)
+    across.pass_on(0, part_ref.at[0], relay_ref, landed_ref)
+    weights.stage3(0)
+    mixed = across.total(0, part_ref.at[0], landed_ref)
+    loads[2 * TILES + 2].wait()
+    middle = (res_ref[...].astype(F32) + rms_scale(mixed, mix_gain_ref[...])).astype(BF16)
+    res_ref[...] = middle
+    normed = rms_scale(middle.astype(F32), pre_gain_ref[...]).astype(BF16)
+    rows_ref[across.rows(tp), :] = normed
+    across.share(rows_ref)
+    weights.stage1(1)
+    weights.stage4(0)
+    across.share_on(rows_ref)
+    weights.stage2(1)
+    weights.stage3(1)
+    across.shared(rows_ref)
+    weights.stage5(0)
+
+    @pl.loop(0, TILES)
+    def _(j):
+        both = dot(rows_ref[...], gu_ref[:, pl.ds(pl.multiple_of(j * 256, 256), 256)])
+        gate, up = both[:, :128], both[:, 128:]
+        hidden = gate / (1.0 + jnp.exp(-gate)) * up
+        hid_ref[pl.ds(pl.multiple_of(j * 128, 128), 128), :] = hidden.T.astype(BF16)
+
+    weights.stage4(1)
+    weights.stage5(1)
+    for h in range(2):
+
+        @pl.loop(0, 4)
+        def _(j):
+            block = dn_ref[pl.ds(pl.multiple_of(h * HALF + j * 256, 256), 256), :]
+            part_ref[1, h, :, pl.ds(pl.multiple_of(j * 256, 256), 256)] = (
+                dot(block, hid_ref[...]).T.astype(BF16))
+
+        if h == 0:
+            across.first(1, part_ref.at[1], relay_ref, landed_ref)
+        else:
+            across.second(1, part_ref.at[1], relay_ref, landed_ref)
+    across.pass_on(1, part_ref.at[1], relay_ref, landed_ref)
+    mixer = across.total(1, part_ref.at[1], landed_ref)
+    merged = res_ref[...].astype(F32) + 0.5 * rms_scale(mixer, post_gain_ref[...])
+    out_ref[...] = merged.astype(BF16)
+    for copy in weights.started + across.started:
+        copy.wait_send()
+
+
+def layer(small, large):
     vmem = pl.BlockSpec(memory_space=pltpu.VMEM)
+    hbm = pl.BlockSpec(memory_space=pl.ANY)
+    dma = pltpu.SemaphoreType.DMA
     return pl.pallas_call(
-        front_kernel,
-        out_shape=jax.ShapeDtypeStruct((T, wo.shape[1]), BF16),
-        in_specs=[vmem] * 10,
+        layer_kernel,
+        out_shape=jax.ShapeDtypeStruct((ROWS, D), BF16),
+        in_specs=[vmem] * len(small) + [hbm] * len(large),
         out_specs=vmem,
         scratch_shapes=[
             pltpu.VMEM((T, GN), F32),
@@ -257,39 +506,23 @@
             pltpu.VMEM((T, 512), BF16),
             pltpu.VMEM((8, 64, 128), F32),
             pltpu.VMEM((4, 64, 128), F32),
-            pltpu.SemaphoreType.DMA((8,)),
-            pltpu.SemaphoreType.DMA((8,)),
-            pltpu.SemaphoreType.DMA((4,)),
-            pltpu.SemaphoreType.DMA((4,)),
+            pltpu.VMEM((512, D), BF16),
+            pltpu.VMEM((ROWS, D), BF16),
+            pltpu.VMEM((D, 2 * F), BF16),
+            pltpu.VMEM((D, F), BF16),
+            pltpu.VMEM((2, 2, T, HALF), BF16),
+            pltpu.VMEM((2, 2, ROWS, HALF), BF16),
+            pltpu.VMEM((2, 2, 2, ROWS, HALF), BF16),
+            pltpu.VMEM((T, D), BF16),
+            pltpu.VMEM((F, T), BF16),
+            dma((8,)), dma((8,)), dma((4,)), dma((4,)),
+            dma((2, 36)), dma((2, 36)), dma((3, 6)), dma((3, 6)), dma((2 * TILES + 3,)),
         ],
         compiler_params=pltpu.CompilerParams(
-            collective_id=0, has_side_effects=True, vmem_limit_bytes=56 * 1024 * 1024
+            collective_id=0, has_side_effects=True, vmem_limit_bytes=66000000
         ),
-        name="front",
-    )(
-        u, a, pr, pi, sl.reshape(1, G), bre.reshape(GN, C), bim.reshape(GN, C),
-        cre.reshape(512, N), cim.reshape(512, N), wo,
-    )
-
-
-def from_everyone(shard, axis):
-    copies = jnp.broadcast_to(shard, (lax.axis_size(axis), *shard.shape))
-    return lax.all_to_all(copies, axis, split_axis=0, concat_axis=0, tiled=True)
-
-
-def summed_on_arrival(shard, axis):
-    count = lax.axis_size(axis)
-    blocks = shard.reshape(count, -1, shard.shape[1])
-    arrived = lax.all_to_all(blocks, axis, split_axis=0, concat_axis=0, tiled=True)
-    return arrived.astype(F32).sum(axis=0)
-
-
-def rms_scale(values, gain):
-    return values * lax.rsqrt(jnp.mean(values * values, axis=-1, keepdims=True) + EPSILON) * gain
-
-
-def round_half(values):
-    return lax.optimization_barrier(values.astype(BF16))
+        name="layer",
+    )(*small, *large)
 
 
 def shards(
@@ -297,24 +530,14 @@
     output_real, output_imaginary, added_log_decay, out_weight, mix_gain, gate_weight, up_weight,
     down_weight, pre_gain, post_gain,
 ):
-    partial = front(
-        ssm_input, added_log_decay, pole_real, pole_imaginary, step_log, input_real,
-        entry_map_quadrature, output_real, output_imaginary, out_weight,
+    small = (
+        ssm_input, added_log_decay.T, pole_real, pole_imaginary, step_log.reshape(1, G),
+        input_real.transpose(0, 2, 1).reshape(512, N),
+        entry_map_quadrature.transpose(0, 2, 1).reshape(512, N),
+        output_real.reshape(512, N), output_imaginary.reshape(512, N),
+        mix_gain.reshape(1, D), pre_gain.reshape(1, D), post_gain.reshape(1, D),
     )
-    mixed_own = summed_on_arrival(partial, "tp")
-    middle = round_half(residual.astype(F32) + rms_scale(mixed_own, mix_gain))
-    normed_own = rms_scale(middle.astype(F32), pre_gain).astype(BF16)
-    mixer_input = from_everyone(normed_own, "tp").reshape(T, -1)
-    both = jnp.concatenate((gate_weight, up_weight, down_weight), axis=1)
-    whole = lax.all_gather(both, "sp", axis=0, tiled=True)
-    f = gate_weight.shape[1]
-    gate_full, up_full, down_full = whole[:, :f], whole[:, f : 2 * f], whole[:, 2 * f :]
-    gate_act = jnp.dot(mixer_input, gate_full, preferred_element_type=F32)
-    up_act = jnp.dot(mixer_input, up_full, preferred_element_type=F32)
-    hidden = (jax.nn.silu(gate_act) * up_act).astype(BF16)
-    mixer_own = summed_on_arrival(dot_nt(hidden, down_full).astype(BF16), "tp")
-    merged = middle.astype(F32) + 0.5 * rms_scale(mixer_own, post_gain)
-    return merged.astype(BF16)
+    return layer(small, (out_weight, residual, gate_weight, up_weight, down_weight))
 
 
 def solution(mesh):

time: 129 us -> 83.6 us (0.65)
  blocking collectives: 53.9 us -> 0 us
  Pallas kernels: 34.5 us -> 81.8 us
  matrix products: 13.7 us -> 0 us
  between operations: 13.5 us -> 0.01 us
  waiting for transfers between devices: 4.1 us -> 0 us
  other arithmetic: 3.92 us -> 0 us
  local copies, waits for them, and re-layouts: 5.31 us -> 1.67 us
    all_to_all x3 -> x0, blocking collectives: 53.9 us -> none  [the longest x2 37.4 us: summed_on_arrival(): lax.all_to_all(blocks, axis, split_axis=0, concat_axis=0, tiled=True)]
    pallas_call x1, Pallas kernels: 34.5 us -> 81.8 us  [layer(): pl.pallas_call(layer_kernel, out_shape=jax.ShapeDtypeStruct((ROWS, D), BF...]
    dot_general x2 -> x0, matrix products: 13.7 us -> none  [the longest x1 8.19 us: dot_nt(): lax.dot_general(a, b, (((1,), (1,)), ((), ())), preferred_element_type=F32)]
    all_gather x1 -> x0, waiting for transfers between devices: 4.09 us -> none  [shards(): whole = lax.all_gather(both, 'sp', axis=0, tiled=True)]
    unnamed x13 -> x1, local copies, waits for them, and re-layouts: 5.2 us -> 1.67 us
    concatenate x1 -> x0, other arithmetic: 1.99 us -> none  [shards(): both = jnp.concatenate((gate_weight, up_weight, down_weight), axis=1)]
  transfers between devices with their start and end apart: 1 -> 0, of which waited for: 1 -> 0; matrix products, arithmetic and copies ran while one was open for 5% -> 0% of each run, Pallas kernels for 27% -> 0%
where the time goes in v1:
time: 83.6 us; the launch traced here: 83.5 us
  Pallas kernels  81.8 us (98%)
  local copies, waits for them, and re-layouts  1.67 us (2%)
    pallas_call x1, Pallas kernels, layer(): pl.pallas_call(layer_kernel, out_shape=jax.ShapeDtypeStruct((ROWS, D), BF...  81.8 us

profile of v1, /device:TPU:1, one launch (start us, length us, event | category | flops | bytes accessed | tf_op | source)
XLA Modules:
  0.0 83.5 jit_solution(6704637233479718350)
XLA Ops:
  0.0 81.8 %layer.1 = bf16[64,2048]{1,0:T(8,128)(2,1)} custom-call(bf16[256,512]{1,0:T(8,128)(2,1)} %u_ref.1, f32[32,256]{1,0:T(8,128)} %bitcast.17, f32[32,64]{1,0:T(8,128)} %pr_ref.1, f32[32,64]{1,0:T(8,128)} %pi_ref.1, f32[1,32]{1,0:T(1,128)} %bitcast.21, f32[512,64]{1,0:T(8,128)} %bitcast.13, f32[512,64]{1,0:T(8,128)} %bitcast.14, f32[512,64]{1,0:T(8,128)} %bitcast.15, ...), custom_call_target="tpu_custom_call" | custom-call | tf_op jit(solution)/shard_map/layer/pallas_call | solution.py:497
  81.8 1.7 %copy.19 = bf16[64,2048]{1,0:T(8,128)(2,1)} copy(bf16[64,2048]{1,0:T(8,128)(2,1)} %layer.1) | data formatting | bytes 524288

commit v2 on v1

--- a/solution.py
+++ b/solution.py
@@ -58,18 +58,20 @@
     return jnp.where(x > -0.5, p * x, jnp.exp(x) - 1.0)
 
 
-def step_rows(pr_ref, pi_ref, sl_ref):
-    tile = one_hot(iota((N, GN), 1) % N == iota((N, GN), 0), F32)
+def lanes_of(v, count):
+    pair = jnp.concatenate([v, v], axis=1)
+    return jnp.concatenate([pair] * (count // 128), axis=1)
+
+
+def step_rows(pr, pi, sl):
     mine = iota((G, GN), 1) // N == iota((G, GN), 0)
-    groups = one_hot(mine, F32)
-
-    def row(ref):
-        wide = dot(ref[...], tile, precision=EXACT)
-        return jnp.sum(jnp.where(mine, wide, 0.0), axis=0, keepdims=True)
-
-    pr, pi = row(pr_ref), row(pi_ref)
-    sl = dot(jnp.broadcast_to(sl_ref[...], (8, G)), groups, precision=EXACT)[0:1]
-    step = jnp.exp(sl)
+
+    def row(v):
+        return jnp.sum(jnp.where(mine, v, 0.0), axis=0, keepdims=True)
+
+    same = iota((G, G), 0) == iota((G, G), 1)
+    column = jnp.sum(jnp.where(same, jnp.broadcast_to(sl, (G, G)), 0.0), axis=1, keepdims=True)
+    pr, pi, step = row(lanes_of(pr, GN)), row(lanes_of(pi, GN)), jnp.exp(row(column))
     log_size = pr * step
     angle = pi * step
     cosine, sine = jnp.cos(angle), jnp.sin(angle)
@@ -80,7 +82,14 @@
     inv = 1.0 / (pr * pr + pi * pi)
     ratio_r = (lift_r * pr + lift_i * pi) * inv
     ratio_i = (lift_i * pr - lift_r * pi) * inv
-    return size * cosine, size * sine, ratio_r, ratio_i, groups
+    return size * cosine, size * sine, ratio_r, ratio_i, mine, row
+
+
+def thirds(v):
+    hi = v.astype(BF16)
+    rest = v - hi.astype(F32)
+    mid = rest.astype(BF16)
+    return jnp.concatenate([hi, mid, (rest - mid.astype(F32)).astype(BF16)], axis=0)
 
 
 def scan_pass(base, e_ref, dr_ref, di_ref, init, store):
@@ -111,16 +120,15 @@
 
 def put_row(ref, slot, part, row):
     for k in range(16):
-        ref[slot, part * 16 + k : part * 16 + k + 1, :] = row[:, k * 128 : (k + 1) * 128]
+        ref[slot, part * 16 + k : part * 16 + k + 1, :] = row[:, k * 128 : (k + 1) * 128].astype(ref.dtype)
+
+
+def to_block(row):
+    return jnp.concatenate([row[:, k * 128 : (k + 1) * 128] for k in range(16)], axis=0)
 
 
 def to_row(block):
     return jnp.concatenate([block[k : k + 1, :] for k in range(16)], axis=1)
-
-
-def parts_of(ref, slot):
-    block = ref[slot]
-    return [block[16 * k : 16 * (k + 1), :] for k in range(4)]
 
 
 def link(first, then):
@@ -182,12 +190,28 @@
     def hand(self, p, k, m):
         self.send(p, 20 + 4 * k + m, self.block(p, k, m), self.partner)
 
+    def along_f(self, p):
+        own = self.block(p, 0, 0)
+        self.send(p, 0, own, self.f_next)
+        self.send(p, 1, own, self.f_prev)
+
+    def beyond_f(self, p):
+        self.arrive(p, 0, self.block(p, 1, 0))
+        self.arrive(p, 1, self.block(p, 2, 0))
+        self.send(p, 2, self.block(p, 1, 0, 0), self.f_next)
+        self.send(p, 3, self.block(p, 2, 0, 1), self.f_prev)
+
+    def opposite_f(self, p):
+        self.arrive(p, 2, self.block(p, 3, 0, 0))
+        self.arrive(p, 3, self.block(p, 3, 0, 1))
+
     def along_s(self, p, k):
         ref = self.block(p, k, 0)
         self.send(p, 4 + 4 * k, ref, self.s_next)
         self.send(p, 5 + 4 * k, ref, self.s_prev)
-
-    def onward(self, p, k):
+        self.hand(p, k, 0)
+
+    def beyond_s(self, p, k):
         self.arrive(p, 4 + 4 * k, self.block(p, k, 1))
         self.arrive(p, 5 + 4 * k, self.block(p, k, 2))
         self.send(p, 6 + 4 * k, self.block(p, k, 1, 0), self.s_next)
@@ -195,47 +219,21 @@
         self.hand(p, k, 1)
         self.hand(p, k, 2)
 
-    def stage0(self, p):
-        own = self.block(p, 0, 0)
-        self.send(p, 0, own, self.f_next)
-        self.send(p, 1, own, self.f_prev)
-        self.along_s(p, 0)
-        self.hand(p, 0, 0)
-
-    def stage1(self, p):
-        self.arrive(p, 0, self.block(p, 1, 0))
-        self.arrive(p, 1, self.block(p, 2, 0))
-        self.send(p, 2, self.block(p, 1, 0, 0), self.f_next)
-        self.send(p, 3, self.block(p, 2, 0, 1), self.f_prev)
-        self.along_s(p, 1)
-        self.hand(p, 1, 0)
-        self.onward(p, 0)
-        self.along_s(p, 2)
-        self.hand(p, 2, 0)
-
-    def stage2(self, p):
-        self.arrive(p, 2, self.block(p, 3, 0, 0))
-        self.arrive(p, 3, self.block(p, 3, 0, 1))
-        self.along_s(p, 3)
-        self.hand(p, 3, 0)
-        self.onward(p, 1)
-
-    def stage3(self, p):
-        self.onward(p, 2)
-        self.onward(p, 3)
-
-    def stage4(self, p):
+    def opposite_s(self, p):
         for k in range(4):
             self.arrive(p, 6 + 4 * k, self.block(p, k, 3, 0))
             self.arrive(p, 7 + 4 * k, self.block(p, k, 3, 1))
             self.hand(p, k, 3)
 
-    def stage5(self, p):
+    def handed(self, p, places):
         for k in range(4):
-            for m in range(4):
+            for m in places:
                 chip = 2 * (self.sk[k] * self.sm + self.fk[m] * self.fm)
                 ref = self.rows(p, (chip + 1 - self.core) * ROWS, None)
                 self.arrive(p, 20 + 4 * k + m, ref)
+
+    def columns(self, k, m):
+        return pl.multiple_of((self.fk[k] * self.fm + self.sk[m] * self.sm) * 128, 128)
 
 
 class Across:
@@ -264,18 +262,21 @@
 
     def first(self, phase, part, relay, landed):
         self.send(phase, 0, part.at[0, self.rows(self.far)], relay.at[phase, 0], self.next)
-        self.send(phase, 3, part.at[0, self.rows(self.prev)], landed.at[phase, 1, 0], self.prev)
+        if phase == 1:
+            self.send(phase, 3, part.at[0, self.rows(self.prev)], landed.at[phase, 1, 0], self.prev)
 
     def second(self, phase, part, relay, landed):
         self.send(phase, 1, part.at[1, self.rows(self.far)], relay.at[phase, 1], self.prev)
+        if phase == 0:
+            self.send(phase, 3, part.at[0, self.rows(self.prev)], landed.at[phase, 1, 0], self.prev)
         self.send(phase, 2, part.at[1, self.rows(self.next)], landed.at[phase, 0, 1], self.next)
 
-    def pass_on(self, phase, part, relay, landed):
-        for side, dev in ((0, self.next), (1, self.prev)):
-            self.arrive(phase, side, relay.at[phase, side])
-            total = relay[phase, side].astype(F32) + part[side, self.rows(dev)].astype(F32)
-            relay[phase, side] = total.astype(BF16)
-            self.send(phase, 4 + side, relay.at[phase, side], landed.at[phase, side, side], dev)
+    def pass_on(self, phase, side, part, relay, landed):
+        dev = (self.next, self.prev)[side]
+        self.arrive(phase, side, relay.at[phase, side])
+        total = relay[phase, side].astype(F32) + part[side, self.rows(dev)].astype(F32)
+        relay[phase, side] = total.astype(BF16)
+        self.send(phase, 4 + side, relay.at[phase, side], landed.at[phase, side, side], dev)
 
     def total(self, phase, part, landed):
         for slot, side, half in ((2, 0, 1), (3, 1, 0), (4, 0, 0), (5, 1, 1)):
@@ -306,13 +307,19 @@
         self.arrive(2, 3, ref.at[self.rows(self.far, 1)])
 
 
+EARLY = [(0, 0), (1, 0), (2, 0), (0, 1), (0, 2), (1, 1), (1, 2), (2, 1)]
+LATE = [(2, 2), (3, 0), (3, 1), (3, 2), (0, 3), (1, 3), (2, 3), (3, 3)]
+
+
 def layer_kernel(
+    u_hbm, a_hbm, pr_hbm, pi_hbm, sl_hbm, bre_hbm, bim_hbm, cre_hbm, cim_hbm,
+    mix_gain_hbm, pre_gain_hbm, post_gain_hbm, wo_hbm, res_hbm, gate_hbm, up_hbm, down_hbm,
+    out_ref,
     u_ref, a_ref, pr_ref, pi_ref, sl_ref, bre_ref, bim_ref, cre_ref, cim_ref,
-    mix_gain_ref, pre_gain_ref, post_gain_ref, wo_hbm, res_hbm, gate_hbm, up_hbm, down_hbm,
-    out_ref,
-    e_ref, dr_ref, di_ref, act_ref, ra_ref, rb_ref, wo_ref, res_ref, gu_ref, dn_ref,
-    part_ref, relay_ref, landed_ref, rows_ref, hid_ref,
-    sa, qa, sb, qb, ws, wq, xs, xq, ls,
+    mix_gain_ref, pre_gain_ref, post_gain_ref, wo_ref, res_ref,
+    e_ref, dr_ref, di_ref, act_ref, cs_ref, ea_ref, eb_ref, ra_ref, rb_ref, gu_ref, dn_ref,
+    part_ref, relay_ref, landed_ref, rows_ref, hid_ref, sum_ref,
+    sa, qa, sb, qb, ws, wq, xs, xq, ls, gs,
 ):
     sp = lax.axis_index("sp")
     tp = lax.axis_index("tp")
@@ -323,50 +330,69 @@
     weights = Gather((gu_ref, dn_ref), ws, wq, sp)
     across = Across(tp, xs, xq)
     own = pl.ds(pl.multiple_of(sp * ROWS, ROWS), ROWS)
-    loads = []
-    for j in range(TILES):
-        for side, hbm in ((0, gate_hbm), (1, up_hbm)):
-            loads.append(pltpu.make_async_copy(
-                hbm.at[:, pl.ds(j * 128, 128)],
-                gu_ref.at[own, pl.ds((2 * j + side) * 128, 128)], ls.at[2 * j + side]))
-    loads.append(pltpu.make_async_copy(down_hbm, dn_ref.at[own], ls.at[2 * TILES]))
-    loads.append(pltpu.make_async_copy(wo_hbm, wo_ref, ls.at[2 * TILES + 1]))
-    loads.append(pltpu.make_async_copy(res_hbm, res_ref, ls.at[2 * TILES + 2]))
-    for load in loads:
-        load.start()
     barrier = pltpu.get_barrier_semaphore()
     for peer in peers_a + peers_b:
         pl.semaphore_signal(barrier, inc=1, device_id={"sp": peer}, device_id_type=MESH)
     for peer in (across.next, across.prev):
         pl.semaphore_signal(barrier, inc=1, device_id={"tp": peer}, device_id_type=MESH)
-    for load in loads[: 2 * TILES]:
+    pairs = (
+        (pr_hbm, pr_ref), (pi_hbm, pi_ref), (sl_hbm, sl_ref), (a_hbm, a_ref), (u_hbm, u_ref),
+        (bre_hbm, bre_ref), (bim_hbm, bim_ref), (cre_hbm, cre_ref), (cim_hbm, cim_ref),
+        (wo_hbm, wo_ref), (res_hbm, res_ref), (mix_gain_hbm, mix_gain_ref),
+        (pre_gain_hbm, pre_gain_ref), (post_gain_hbm, post_gain_ref), (down_hbm, dn_ref.at[own]),
+    )
+    loads = [pltpu.make_async_copy(src, dst, ls.at[k]) for k, (src, dst) in enumerate(pairs)]
+    for load in loads[:4]:
+        load.start()
+    shard_loads = []
+    for j in range(TILES):
+        for side, hbm in ((0, gate_hbm), (1, up_hbm)):
+            shard_loads.append(pltpu.make_async_copy(
+                hbm.at[:, pl.ds(j * 128, 128)],
+                gu_ref.at[own, pl.ds((2 * j + side) * 128, 128)], gs.at[2 * j + side]))
+            shard_loads[-1].start()
+    for load in loads[4:]:
+        load.start()
+    for load in loads[:4]:
+        load.wait()
+
+    base_r, base_i, ratio_r, ratio_i, mine, row = step_rows(pr_ref[...], pi_ref[...], sl_ref[...])
+    ea_row = jnp.exp(row(jnp.sum(a_ref[...], axis=1, keepdims=True)))
+    put_row(ea_ref, 0, 0, ea_row)
+    for load in shard_loads:
         load.wait()
     pl.semaphore_wait(barrier, 12)
-    weights.stage0(0)
-
-    base_r, base_i, ratio_r, ratio_i, groups = step_rows(pr_ref, pi_ref, sl_ref)
+    early = []
+    for d in range(1, 8):
+        early.append(pltpu.make_async_remote_copy(
+            ea_ref.at[0], ea_ref.at[d], sa.at[0, d], qa.at[0, d],
+            device_id={"sp": peers_a[d - 1]}, device_id_type=MESH))
+        early[-1].start()
+    weights.along_f(0)
+
     perm = iota((T, T), 0) == (iota((T, T), 1) % SEGS) * STEPS + iota((T, T), 1) // SEGS
-    e_small = dot(jnp.exp(a_ref[...]), one_hot(perm, F32), precision=EXACT)
+    order = iota((T, T), 1) == (iota((T, T), 0) % SEGS) * STEPS + iota((T, T), 0) // SEGS
+    e_small = dot(thirds(jnp.exp(a_ref[...])), one_hot(perm, BF16)).astype(BF16)
+    groups = one_hot(mine, BF16)
     e_ref[...] = lax.dot_general(
-        e_small, groups, (((0,), (0,)), ((), ())), precision=EXACT, preferred_element_type=F32)
-    order = iota((T, T), 1) == (iota((T, T), 0) % SEGS) * STEPS + iota((T, T), 0) // SEGS
+        e_small, jnp.concatenate([groups] * 3, axis=0), (((0,), (0,)), ((), ())),
+        preferred_element_type=F32)
+    for load in loads[4:9]:
+        load.wait()
     u = dot(one_hot(order, BF16), u_ref[...]).astype(BF16)
-    lay = one_hot(iota((N, 1024), 1) % N == iota((N, 1024), 0), BF16)
     inside = iota((256, 1024), 0) // C == iota((256, 1024), 1) // N
 
     def spread(v):
-        return [jnp.where(inside, dot(piece, lay), 0.0).astype(BF16) for piece in split(v)]
+        return jnp.where(inside, lanes_of(v, 1024), 0.0).astype(BF16)
 
     for h in range(2):
         gn = slice(h * 1024, (h + 1) * 1024)
         ch = slice(h * 256, (h + 1) * 256)
-        raw = []
-        for ref in (bre_ref, bim_ref):
-            hi, lo = spread(ref[ch, :])
-            raw.append(dot(u[:, ch], hi) + dot(u[:, ch], lo))
+        raw_r = dot(u[:, ch], spread(bre_ref[ch, :]))
+        raw_i = dot(u[:, ch], spread(bim_ref[ch, :]))
         rr, ri = ratio_r[:, gn], ratio_i[:, gn]
-        dr_ref[:, gn] = rr * raw[0] - ri * raw[1]
-        di_ref[:, gn] = rr * raw[1] + ri * raw[0]
+        dr_ref[:, gn] = rr * raw_r - ri * raw_i
+        di_ref[:, gn] = rr * raw_i + ri * raw_r
 
     zero = jnp.zeros((SEGS, GN), F32)
     end_r, end_i, pe = scan_pass((base_r, base_i), e_ref, dr_ref, di_ref, (zero, zero), False)
@@ -381,42 +407,74 @@
     for j in range(SEGS):
         before.append(total)
         total = link(total, (seg_r[j : j + 1], seg_i[j : j + 1], end_r[j : j + 1], end_i[j : j + 1]))
-    for k in range(4):
-        put_row(ra_ref, 0, k, total[k])
-
-    copies = []
+    put_row(ra_ref, 0, 0, total[2])
+    put_row(ra_ref, 0, 1, total[3])
+
+    sent_a = []
     for d in range(1, 8):
-        copies.append(pltpu.make_async_remote_copy(
-            ra_ref.at[0], ra_ref.at[d], sa.at[d], qa.at[d],
+        sent_a.append(pltpu.make_async_remote_copy(
+            ra_ref.at[0], ra_ref.at[d], sa.at[1, d], qa.at[1, d],
             device_id={"sp": peers_a[d - 1]}, device_id_type=MESH))
-        copies[-1].start()
-    for copy in copies:
+        sent_a[-1].start()
+    loads[14].wait()
+    weights.along_f(1)
+    for h in range(2):
+        ch = slice(h * 256, (h + 1) * 256)
+        cs_ref[h, 0] = spread(cre_ref[ch, :])
+        cs_ref[h, 1] = spread(-cim_ref[ch, :])
+    w_r, w_i = to_block(wr), to_block(wi)
+    for _ in range(3):
+        w_r, w_i = cmul(w_r, w_i, w_r, w_i)
+    v_r, v_i = w_r, w_i
+    for _ in range(3):
+        v_r, v_i = cmul(v_r, v_i, v_r, v_i)
+    for copy in early:
+        copy.wait()
+    eb = ea_ref[0]
+    for d in range(1, 8):
+        eb = eb * ea_ref[d]
+    eb_ref[0] = eb
+    early_b = []
+    for d in range(1, 4):
+        early_b.append(pltpu.make_async_remote_copy(
+            eb_ref.at[0], eb_ref.at[d], sb.at[0, d], qb.at[0, d],
+            device_id={"sp": peers_b[d - 1]}, device_id_type=MESH))
+        early_b[-1].start()
+    for copy in sent_a:
         copy.wait()
     unit = jnp.ones((16, 128), F32)
     null = jnp.zeros((16, 128), F32)
+
+    def stretch(e, pr, pi, ref, slot):
+        block = ref[slot].astype(F32)
+        decay = e[slot]
+        return pr * decay, pi * decay, block[:16], block[16:]
+
     run = (unit, null, null, null)
     pre_a = run
     for k in range(8):
         pre_a = choose(q == k, run, pre_a)
-        run = link(run, parts_of(ra_ref, (q - k + 8) % 8))
-    for k in range(4):
-        rb_ref[0, 16 * k : 16 * (k + 1), :] = run[k]
-    copies = []
+        run = link(run, stretch(ea_ref, w_r, w_i, ra_ref, (q - k + 8) % 8))
+    rb_ref[0, :16] = run[2].astype(BF16)
+    rb_ref[0, 16:] = run[3].astype(BF16)
+    sent_b = []
     for d in range(1, 4):
-        copies.append(pltpu.make_async_remote_copy(
-            rb_ref.at[0], rb_ref.at[d], sb.at[d], qb.at[d],
+        sent_b.append(pltpu.make_async_remote_copy(
+            rb_ref.at[0], rb_ref.at[d], sb.at[1, d], qb.at[1, d],
             device_id={"sp": peers_b[d - 1]}, device_id_type=MESH))
-        copies[-1].start()
-    weights.stage1(0)
-    loads[2 * TILES].wait()
-    weights.stage0(1)
-    for copy in copies:
+        sent_b[-1].start()
+    weights.along_s(0, 0)
+    weights.beyond_f(0)
+    weights.along_s(0, 1)
+    weights.along_s(0, 2)
+    weights.beyond_f(1)
+    for copy in early_b + sent_b:
         copy.wait()
     run = (unit, null, null, null)
     pre_b = run
     for k in range(4):
         pre_b = choose(z == k, run, pre_b)
-        run = link(run, parts_of(rb_ref, (z - k + 4) % 4))
+        run = link(run, stretch(eb_ref, v_r, v_i, rb_ref, (z - k + 4) % 4))
     carry = link(pre_b, pre_a)
     cr, ci = to_row(carry[2]), to_row(carry[3])
     starts = []
@@ -429,85 +487,98 @@
 
     for h in range(2):
         gn = slice(h * 1024, (h + 1) * 1024)
-        ch = slice(h * 256, (h + 1) * 256)
-        y = None
-        for s_ref, c_ref, sign in ((dr_ref, cre_ref, 1.0), (di_ref, cim_ref, -1.0)):
-            s_hi, s_lo = split(s_ref[:, gn])
-            c_hi, c_lo = spread(sign * c_ref[ch, :])
-            term = dot_nt(s_hi, c_hi) + dot_nt(s_lo, c_hi) + dot_nt(s_hi, c_lo)
-            y = term if y is None else y + term
-        act_ref[:, ch] = jax.nn.gelu(y).astype(BF16)
+        y = dot_nt(dr_ref[:, gn].astype(BF16), cs_ref[h, 0])
+        y = y + dot_nt(di_ref[:, gn].astype(BF16), cs_ref[h, 1])
+        act_ref[:, h * 256 : (h + 1) * 256] = jax.nn.gelu(y).astype(BF16)
     act = dot(one_hot(perm, BF16), act_ref[...]).astype(BF16)
-    loads[2 * TILES + 1].wait()
+    loads[9].wait()
     part_ref[0, 0] = dot(act, wo_ref[:, :HALF]).astype(BF16)
     across.first(0, part_ref.at[0], relay_ref, landed_ref)
     part_ref[0, 1] = dot(act, wo_ref[:, HALF:]).astype(BF16)
     across.second(0, part_ref.at[0], relay_ref, landed_ref)
-    weights.stage2(0)
-    across.pass_on(0, part_ref.at[0], relay_ref, landed_ref)
-    weights.stage3(0)
+    weights.opposite_f(0)
+    weights.along_s(0, 3)
+    weights.beyond_s(0, 0)
+    across.pass_on(0, 0, part_ref.at[0], relay_ref, landed_ref)
+    across.pass_on(0, 1, part_ref.at[0], relay_ref, landed_ref)
+    weights.beyond_s(0, 1)
     mixed = across.total(0, part_ref.at[0], landed_ref)
-    loads[2 * TILES + 2].wait()
+    for load in loads[10:14]:
+        load.wait()
     middle = (res_ref[...].astype(F32) + rms_scale(mixed, mix_gain_ref[...])).astype(BF16)
     res_ref[...] = middle
     normed = rms_scale(middle.astype(F32), pre_gain_ref[...]).astype(BF16)
     rows_ref[across.rows(tp), :] = normed
     across.share(rows_ref)
-    weights.stage1(1)
-    weights.stage4(0)
+    weights.beyond_s(0, 2)
+    weights.opposite_f(1)
+    weights.along_s(1, 0)
+    weights.along_s(1, 1)
     across.share_on(rows_ref)
-    weights.stage2(1)
-    weights.stage3(1)
+    weights.beyond_s(0, 3)
+    weights.along_s(1, 2)
+    weights.along_s(1, 3)
     across.shared(rows_ref)
-    weights.stage5(0)
-
-    @pl.loop(0, TILES)
-    def _(j):
-        both = dot(rows_ref[...], gu_ref[:, pl.ds(pl.multiple_of(j * 256, 256), 256)])
+    weights.opposite_s(0)
+    weights.handed(0, range(4))
+    for j in range(TILES):
+        both = dot(rows_ref[...], gu_ref[:, j * 256 : (j + 1) * 256])
         gate, up = both[:, :128], both[:, 128:]
         hidden = gate / (1.0 + jnp.exp(-gate)) * up
-        hid_ref[pl.ds(pl.multiple_of(j * 128, 128), 128), :] = hidden.T.astype(BF16)
-
-    weights.stage4(1)
-    weights.stage5(1)
-    for h in range(2):
-
-        @pl.loop(0, 4)
-        def _(j):
-            block = dn_ref[pl.ds(pl.multiple_of(h * HALF + j * 256, 256), 256), :]
-            part_ref[1, h, :, pl.ds(pl.multiple_of(j * 256, 256), 256)] = (
-                dot(block, hid_ref[...]).T.astype(BF16))
-
+        hid_ref[j * 128 : (j + 1) * 128, :] = hidden.T.astype(BF16)
+        if j == 5:
+            weights.beyond_s(1, 0)
+            weights.beyond_s(1, 1)
+
+    weights.beyond_s(1, 2)
+    weights.beyond_s(1, 3)
+    weights.handed(1, range(3))
+    for h, chips in enumerate((EARLY, LATE)):
+        if h == 1:
+            weights.opposite_s(1)
+            weights.handed(1, (3,))
+            across.pass_on(1, 0, part_ref.at[1], relay_ref, landed_ref)
+        for j in (0, 4):
+            block = jnp.concatenate(
+                [dn_ref[pl.ds(weights.columns(k, m), 128), :] for k, m in chips[j : j + 4]], axis=0)
+            out = dot(block, hid_ref[...])
+            for i in range(4):
+                part_ref[1, h, :, (j + i) * 128 : (j + i + 1) * 128] = (
+                    out[i * 128 : (i + 1) * 128].T.astype(BF16))
         if h == 0:
             across.first(1, part_ref.at[1], relay_ref, landed_ref)
         else:
             across.second(1, part_ref.at[1], relay_ref, landed_ref)
-    across.pass_on(1, part_ref.at[1], relay_ref, landed_ref)
+    across.pass_on(1, 1, part_ref.at[1], relay_ref, landed_ref)
     mixer = across.total(1, part_ref.at[1], landed_ref)
-    merged = res_ref[...].astype(F32) + 0.5 * rms_scale(mixer, post_gain_ref[...])
+    for j, (k, m) in enumerate(EARLY + LATE):
+        sum_ref[:, pl.ds(weights.columns(k, m), 128)] = mixer[:, j * 128 : (j + 1) * 128]
+    merged = res_ref[...].astype(F32) + 0.5 * rms_scale(sum_ref[...], post_gain_ref[...])
     out_ref[...] = merged.astype(BF16)
     for copy in weights.started + across.started:
         copy.wait_send()
 
 
-def layer(small, large):
-    vmem = pl.BlockSpec(memory_space=pltpu.VMEM)
+def layer(arrays):
     hbm = pl.BlockSpec(memory_space=pl.ANY)
     dma = pltpu.SemaphoreType.DMA
+    held = [pltpu.VMEM(v.shape, v.dtype) for v in arrays[:14]]
     return pl.pallas_call(
         layer_kernel,
         out_shape=jax.ShapeDtypeStruct((ROWS, D), BF16),
-        in_specs=[vmem] * len(small) + [hbm] * len(large),
-        out_specs=vmem,
+        in_specs=[hbm] * len(arrays),
+        out_specs=pl.BlockSpec(memory_space=pltpu.VMEM),
         scratch_shapes=[
+            *held,
             pltpu.VMEM((T, GN), F32),
             pltpu.VMEM((T, GN), F32),
             pltpu.VMEM((T, GN), F32),
             pltpu.VMEM((T, 512), BF16),
-            pltpu.VMEM((8, 64, 128), F32),
-            pltpu.VMEM((4, 64, 128), F32),
-            pltpu.VMEM((512, D), BF16),
-            pltpu.VMEM((ROWS, D), BF16),
+            pltpu.VMEM((2, 2, 256, 1024), BF16),
+            pltpu.VMEM((8, 16, 128), F32),
+            pltpu.VMEM((4, 16, 128), F32),
+            pltpu.VMEM((8, 32, 128), BF16),
+            pltpu.VMEM((4, 32, 128), BF16),
             pltpu.VMEM((D, 2 * F), BF16),
             pltpu.VMEM((D, F), BF16),
             pltpu.VMEM((2, 2, T, HALF), BF16),
@@ -515,14 +586,15 @@
             pltpu.VMEM((2, 2, 2, ROWS, HALF), BF16),
             pltpu.VMEM((T, D), BF16),
             pltpu.VMEM((F, T), BF16),
-            dma((8,)), dma((8,)), dma((4,)), dma((4,)),
-            dma((2, 36)), dma((2, 36)), dma((3, 6)), dma((3, 6)), dma((2 * TILES + 3,)),
+            pltpu.VMEM((ROWS, D), F32),
+            dma((2, 8)), dma((2, 8)), dma((2, 4)), dma((2, 4)),
+            dma((2, 36)), dma((2, 36)), dma((3, 6)), dma((3, 6)), dma((15,)), dma((2 * TILES,)),
         ],
         compiler_params=pltpu.CompilerParams(
             collective_id=0, has_side_effects=True, vmem_limit_bytes=66000000
         ),
         name="layer",
-    )(*small, *large)
+    )(*arrays)
 
 
 def shards(
@@ -537,7 +609,7 @@
         output_real.reshape(512, N), output_imaginary.reshape(512, N),
         mix_gain.reshape(1, D), pre_gain.reshape(1, D), post_gain.reshape(1, D),
     )
-    return layer(small, (out_weight, residual, gate_weight, up_weight, down_weight))
+    return layer(small + (out_weight, residual, gate_weight, up_weight, down_weight))
 
 
 def solution(mesh):

time: 83.6 us -> 76.2 us (0.911)
  the two profiles are of different devices: /device:TPU:1 before, /device:TPU:4 now
where the time goes in v2:
time: 76.2 us; the launch traced here: 76.1 us
  Pallas kernels  74.4 us (98%)
  local copies, waits for them, and re-layouts  1.67 us (2%)
    pallas_call x1, Pallas kernels, layer(): pl.pallas_call(layer_kernel, out_shape=jax.ShapeDtypeStruct((ROWS, D), BF...  74.4 us
    unnamed x1, local copies, waits for them, and re-layouts  1.67 us

profile of v2, /device:TPU:4, one launch (start us, length us, event | category | flops | bytes accessed | tf_op | source)
XLA Modules:
  0.0 76.1 jit_solution(9240797250239201437)
XLA Ops:
  0.0 74.4 %layer.1 = bf16[64,2048]{1,0:T(8,128)(2,1)} custom-call(bf16[256,512]{1,0:T(8,128)(2,1)} %u_hbm.1, f32[32,256]{1,0:T(8,128)} %bitcast.17, f32[32,64]{1,0:T(8,128)} %pr_hbm.1, f32[32,64]{1,0:T(8,128)} %pi_hbm.1, f32[1,32]{1,0:T(1,128)} %bitcast.21, f32[512,64]{1,0:T(8,128)} %bitcast.13, f32[512,64]{1,0:T(8,128)} %bitcast.14, f32[512,64]{1,0:T(8,128)} %bitcast.15, ...), custom_call_target="tpu_custom_call" | custom-call | tf_op jit(solution)/shard_map/layer/pallas_call | solution.py:566
  74.4 1.7 %copy.19 = bf16[64,2048]{1,0:T(8,128)(2,1)} copy(bf16[64,2048]{1,0:T(8,128)(2,1)} %layer.1) | data formatting | bytes 524288

commit v3 on v2

--- a/solution.py
+++ b/solution.py
@@ -190,16 +190,40 @@
     def hand(self, p, k, m):
         self.send(p, 20 + 4 * k + m, self.block(p, k, m), self.partner)
 
-    def along_f(self, p):
-        own = self.block(p, 0, 0)
-        self.send(p, 0, own, self.f_next)
-        self.send(p, 1, own, self.f_prev)
+    def own_along(self, p, turn, half):
+        own = self.block(p, 0, 0, half)
+        nexts, prevs = (self.f_next, self.s_next), (self.f_prev, self.s_prev)
+        for side, (f_dev, s_dev) in enumerate((nexts, prevs)):
+            f_slot, s_slot = side, 4 + side
+            if half:
+                f_slot, s_slot = 36 + side, 38 + side
+            self.send(p, f_slot + turn * (s_slot - f_slot), own, f_dev + turn * (s_dev - f_dev))
 
     def beyond_f(self, p):
         self.arrive(p, 0, self.block(p, 1, 0))
         self.arrive(p, 1, self.block(p, 2, 0))
         self.send(p, 2, self.block(p, 1, 0, 0), self.f_next)
         self.send(p, 3, self.block(p, 2, 0, 1), self.f_prev)
+
+    def beyond_f_next(self):
+        self.arrive(0, 0, self.block(0, 1, 0, 0))
+        self.send(0, 2, self.block(0, 1, 0, 0), self.f_next)
+
+    def beyond_f_prev(self):
+        self.arrive(0, 37, self.block(0, 2, 0, 1))
+        self.send(0, 3, self.block(0, 2, 0, 1), self.f_prev)
+        self.arrive(0, 36, self.block(0, 1, 0, 1))
+        self.arrive(0, 1, self.block(0, 2, 0, 0))
+
+    def beyond_s_own(self):
+        self.arrive(0, 4, self.block(0, 0, 1, 0))
+        self.arrive(0, 39, self.block(0, 0, 2, 1))
+        self.send(0, 6, self.block(0, 0, 1, 0), self.s_next)
+        self.send(0, 7, self.block(0, 0, 2, 1), self.s_prev)
+        self.arrive(0, 38, self.block(0, 0, 1, 1))
+        self.arrive(0, 5, self.block(0, 0, 2, 0))
+        self.hand(0, 0, 1)
+        self.hand(0, 0, 2)
 
     def opposite_f(self, p):
         self.arrive(p, 2, self.block(p, 3, 0, 0))
@@ -226,11 +250,10 @@
             self.hand(p, k, 3)
 
     def handed(self, p, places):
-        for k in range(4):
-            for m in places:
-                chip = 2 * (self.sk[k] * self.sm + self.fk[m] * self.fm)
-                ref = self.rows(p, (chip + 1 - self.core) * ROWS, None)
-                self.arrive(p, 20 + 4 * k + m, ref)
+        for k, m in places:
+            chip = 2 * (self.sk[k] * self.sm + self.fk[m] * self.fm)
+            ref = self.rows(p, (chip + 1 - self.core) * ROWS, None)
+            self.arrive(p, 20 + 4 * k + m, ref)
 
     def columns(self, k, m):
         return pl.multiple_of((self.fk[k] * self.fm + self.sk[m] * self.sm) * 128, 128)
@@ -260,53 +283,54 @@
             return pl.ds(pl.multiple_of(x * ROWS, ROWS), ROWS)
         return pl.ds(pl.multiple_of(x * ROWS + half * 32, 32), 32)
 
-    def first(self, phase, part, relay, landed):
-        self.send(phase, 0, part.at[0, self.rows(self.far)], relay.at[phase, 0], self.next)
-        if phase == 1:
-            self.send(phase, 3, part.at[0, self.rows(self.prev)], landed.at[phase, 1, 0], self.prev)
-
-    def second(self, phase, part, relay, landed):
-        self.send(phase, 1, part.at[1, self.rows(self.far)], relay.at[phase, 1], self.prev)
-        if phase == 0:
-            self.send(phase, 3, part.at[0, self.rows(self.prev)], landed.at[phase, 1, 0], self.prev)
-        self.send(phase, 2, part.at[1, self.rows(self.next)], landed.at[phase, 0, 1], self.next)
-
-    def pass_on(self, phase, side, part, relay, landed):
-        dev = (self.next, self.prev)[side]
-        self.arrive(phase, side, relay.at[phase, side])
-        total = relay[phase, side].astype(F32) + part[side, self.rows(dev)].astype(F32)
-        relay[phase, side] = total.astype(BF16)
-        self.send(phase, 4 + side, relay.at[phase, side], landed.at[phase, side, side], dev)
-
-    def total(self, phase, part, landed):
-        for slot, side, half in ((2, 0, 1), (3, 1, 0), (4, 0, 0), (5, 1, 1)):
-            self.arrive(phase, slot, landed.at[phase, side, half])
-        halves = [
-            part[h, self.rows(self.x)].astype(F32)
-            + landed[phase, 0, h].astype(F32)
-            + landed[phase, 1, h].astype(F32)
-            for h in range(2)
+    def start_sum(self, phase, g, part, relay, landed):
+        self.send(phase, 6 * g, part.at[g, 0, self.rows(self.far)], relay.at[phase, g, 0], self.next)
+        self.send(phase, 6 * g + 1, part.at[g, 1, self.rows(self.far)], relay.at[phase, g, 1], self.prev)
+        self.send(
+            phase, 6 * g + 2, part.at[g, 1, self.rows(self.next)], landed.at[phase, g, 0, 1], self.next)
+        self.send(
+            phase, 6 * g + 3, part.at[g, 0, self.rows(self.prev)], landed.at[phase, g, 1, 0], self.prev)
+
+    def pass_on(self, phase, g, part, relay, landed):
+        for side, dev in ((0, self.next), (1, self.prev)):
+            self.arrive(phase, 6 * g + side, relay.at[phase, g, side])
+            total = relay[phase, g, side].astype(F32) + part[g, side, self.rows(dev)].astype(F32)
+            relay[phase, g, side] = total.astype(BF16)
+            self.send(
+                phase, 6 * g + 4 + side, relay.at[phase, g, side], landed.at[phase, g, side, side], dev)
+
+    def total(self, phase, g, part, landed):
+        for slot, side, sub in ((2, 0, 1), (3, 1, 0), (4, 0, 0), (5, 1, 1)):
+            self.arrive(phase, 6 * g + slot, landed.at[phase, g, side, sub])
+        return [
+            part[g, sub, self.rows(self.x)].astype(F32)
+            + landed[phase, g, 0, sub].astype(F32)
+            + landed[phase, g, 1, sub].astype(F32)
+            for sub in range(2)
         ]
-        return jnp.concatenate(halves, axis=1)
 
     def share(self, ref):
-        own = ref.at[self.rows(self.x)]
-        self.send(2, 0, own, own, self.next)
-        self.send(2, 1, own, own, self.prev)
+        top, bottom = (ref.at[self.rows(self.x, half)] for half in range(2))
+        self.send(2, 0, top, top, self.next)
+        self.send(2, 1, bottom, bottom, self.prev)
+        self.send(2, 6, bottom, bottom, self.next)
+        self.send(2, 7, top, top, self.prev)
 
     def share_on(self, ref):
-        self.arrive(2, 0, ref.at[self.rows(self.prev)])
-        self.arrive(2, 1, ref.at[self.rows(self.next)])
-        top = ref.at[self.rows(self.prev, 0)]
-        bottom = ref.at[self.rows(self.next, 1)]
+        top, bottom = ref.at[self.rows(self.prev, 0)], ref.at[self.rows(self.next, 1)]
+        self.arrive(2, 0, top)
         self.send(2, 2, top, top, self.next)
+        self.arrive(2, 1, bottom)
         self.send(2, 3, bottom, bottom, self.prev)
 
     def shared(self, ref):
+        self.arrive(2, 6, ref.at[self.rows(self.prev, 1)])
+        self.arrive(2, 7, ref.at[self.rows(self.next, 0)])
         self.arrive(2, 2, ref.at[self.rows(self.far, 0)])
         self.arrive(2, 3, ref.at[self.rows(self.far, 1)])
 
 
+QUARTER = D // 4
 EARLY = [(0, 0), (1, 0), (2, 0), (0, 1), (0, 2), (1, 1), (1, 2), (2, 1)]
 LATE = [(2, 2), (3, 0), (3, 1), (3, 2), (0, 3), (1, 3), (2, 3), (3, 3)]
 
@@ -330,6 +354,12 @@
     weights = Gather((gu_ref, dn_ref), ws, wq, sp)
     across = Across(tp, xs, xq)
     own = pl.ds(pl.multiple_of(sp * ROWS, ROWS), ROWS)
+    shard_loads = [
+        pltpu.make_async_copy(hbm, gu_ref.at[own, pl.ds(side * F, F)], gs.at[side])
+        for side, hbm in enumerate((gate_hbm, up_hbm))
+    ]
+    for load in shard_loads:
+        load.start()
     barrier = pltpu.get_barrier_semaphore()
     for peer in peers_a + peers_b:
         pl.semaphore_signal(barrier, inc=1, device_id={"sp": peer}, device_id_type=MESH)
@@ -344,31 +374,27 @@
     loads = [pltpu.make_async_copy(src, dst, ls.at[k]) for k, (src, dst) in enumerate(pairs)]
     for load in loads[:4]:
         load.start()
-    shard_loads = []
-    for j in range(TILES):
-        for side, hbm in ((0, gate_hbm), (1, up_hbm)):
-            shard_loads.append(pltpu.make_async_copy(
-                hbm.at[:, pl.ds(j * 128, 128)],
-                gu_ref.at[own, pl.ds((2 * j + side) * 128, 128)], gs.at[2 * j + side]))
-            shard_loads[-1].start()
     for load in loads[4:]:
         load.start()
+    for load in shard_loads:
+        load.wait()
+    pl.semaphore_wait(barrier, 12)
+    weights.own_along(0, weights.core, 0)
+    weights.own_along(0, 1 - weights.core, 0)
+    weights.own_along(0, 1 - weights.core, 1)
+    weights.hand(0, 0, 0)
     for load in loads[:4]:
         load.wait()
 
     base_r, base_i, ratio_r, ratio_i, mine, row = step_rows(pr_ref[...], pi_ref[...], sl_ref[...])
     ea_row = jnp.exp(row(jnp.sum(a_ref[...], axis=1, keepdims=True)))
     put_row(ea_ref, 0, 0, ea_row)
-    for load in shard_loads:
-        load.wait()
-    pl.semaphore_wait(barrier, 12)
     early = []
     for d in range(1, 8):
         early.append(pltpu.make_async_remote_copy(
             ea_ref.at[0], ea_ref.at[d], sa.at[0, d], qa.at[0, d],
             device_id={"sp": peers_a[d - 1]}, device_id_type=MESH))
         early[-1].start()
-    weights.along_f(0)
 
     perm = iota((T, T), 0) == (iota((T, T), 1) % SEGS) * STEPS + iota((T, T), 1) // SEGS
     order = iota((T, T), 1) == (iota((T, T), 0) % SEGS) * STEPS + iota((T, T), 0) // SEGS
@@ -416,8 +442,10 @@
             ra_ref.at[0], ra_ref.at[d], sa.at[1, d], qa.at[1, d],
             device_id={"sp": peers_a[d - 1]}, device_id_type=MESH))
         sent_a[-1].start()
+    weights.own_along(0, weights.core, 1)
     loads[14].wait()
-    weights.along_f(1)
+    weights.own_along(1, weights.core, None)
+    weights.hand(1, 0, 0)
     for h in range(2):
         ch = slice(h * 256, (h + 1) * 256)
         cs_ref[h, 0] = spread(cre_ref[ch, :])
@@ -463,11 +491,11 @@
             rb_ref.at[0], rb_ref.at[d], sb.at[1, d], qb.at[1, d],
             device_id={"sp": peers_b[d - 1]}, device_id_type=MESH))
         sent_b[-1].start()
-    weights.along_s(0, 0)
-    weights.beyond_f(0)
+    weights.own_along(1, 1 - weights.core, None)
+    weights.beyond_f_next()
+    weights.beyond_f_prev()
     weights.along_s(0, 1)
     weights.along_s(0, 2)
-    weights.beyond_f(1)
     for copy in early_b + sent_b:
         copy.wait()
     run = (unit, null, null, null)
@@ -492,17 +520,21 @@
         act_ref[:, h * 256 : (h + 1) * 256] = jax.nn.gelu(y).astype(BF16)
     act = dot(one_hot(perm, BF16), act_ref[...]).astype(BF16)
     loads[9].wait()
-    part_ref[0, 0] = dot(act, wo_ref[:, :HALF]).astype(BF16)
-    across.first(0, part_ref.at[0], relay_ref, landed_ref)
-    part_ref[0, 1] = dot(act, wo_ref[:, HALF:]).astype(BF16)
-    across.second(0, part_ref.at[0], relay_ref, landed_ref)
+    for g in range(2):
+        out = dot(act, wo_ref[:, g * HALF : (g + 1) * HALF]).astype(BF16)
+        part_ref[0, g, 0] = out[:, :QUARTER]
+        part_ref[0, g, 1] = out[:, QUARTER:]
+        across.start_sum(0, g, part_ref.at[0], relay_ref, landed_ref)
+    weights.beyond_s_own()
+    across.pass_on(0, 0, part_ref.at[0], relay_ref, landed_ref)
     weights.opposite_f(0)
     weights.along_s(0, 3)
-    weights.beyond_s(0, 0)
-    across.pass_on(0, 0, part_ref.at[0], relay_ref, landed_ref)
     across.pass_on(0, 1, part_ref.at[0], relay_ref, landed_ref)
     weights.beyond_s(0, 1)
-    mixed = across.total(0, part_ref.at[0], landed_ref)
+    weights.beyond_f(1)
+    mixed = jnp.concatenate(
+        across.total(0, 0, part_ref.at[0], landed_ref)
+        + across.total(0, 1, part_ref.at[0], landed_ref), axis=1)
     for load in loads[10:14]:
         load.wait()
     middle = (res_ref[...].astype(F32) + rms_scale(mixed, mix_gain_ref[...])).astype(BF16)
@@ -511,50 +543,53 @@
     rows_ref[across.rows(tp), :] = normed
     across.share(rows_ref)
     weights.beyond_s(0, 2)
-    weights.opposite_f(1)
-    weights.along_s(1, 0)
-    weights.along_s(1, 1)
     across.share_on(rows_ref)
     weights.beyond_s(0, 3)
+    weights.along_s(1, 1)
     weights.along_s(1, 2)
+    weights.opposite_f(1)
     weights.along_s(1, 3)
+    weights.beyond_s(1, 0)
     across.shared(rows_ref)
     weights.opposite_s(0)
-    weights.handed(0, range(4))
-    for j in range(TILES):
-        both = dot(rows_ref[...], gu_ref[:, j * 256 : (j + 1) * 256])
-        gate, up = both[:, :128], both[:, 128:]
+    weights.handed(0, [(k, m) for k in range(4) for m in range(4)])
+    def hidden_tile(gate, up, first):
         hidden = gate / (1.0 + jnp.exp(-gate)) * up
-        hid_ref[j * 128 : (j + 1) * 128, :] = hidden.T.astype(BF16)
-        if j == 5:
-            weights.beyond_s(1, 0)
+        hid_ref[first : first + gate.shape[1], :] = hidden.T.astype(BF16)
+
+    for first in range(0, F - 128, 256):
+        tile = [gu_ref[:, side * F + first : side * F + first + 256] for side in range(2)]
+        hidden_tile(dot(rows_ref[...], tile[0]), dot(rows_ref[...], tile[1]), first)
+        if first == 512:
             weights.beyond_s(1, 1)
+    both = dot(rows_ref[...], jnp.concatenate([gu_ref[:, F - 128 : F], gu_ref[:, 2 * F - 128 :]], axis=1))
+    hidden_tile(both[:, :128], both[:, 128:], F - 128)
 
     weights.beyond_s(1, 2)
     weights.beyond_s(1, 3)
-    weights.handed(1, range(3))
-    for h, chips in enumerate((EARLY, LATE)):
-        if h == 1:
+    weights.handed(1, [(k, m) for k in range(3) for m in range(3)])
+    for g, chips in enumerate((EARLY, LATE)):
+        if g == 1:
             weights.opposite_s(1)
-            weights.handed(1, (3,))
+            weights.handed(1, [(k, m) for k in range(4) for m in range(4) if k == 3 or m == 3])
             across.pass_on(1, 0, part_ref.at[1], relay_ref, landed_ref)
-        for j in (0, 4):
+        for sub in range(2):
             block = jnp.concatenate(
-                [dn_ref[pl.ds(weights.columns(k, m), 128), :] for k, m in chips[j : j + 4]], axis=0)
+                [dn_ref[pl.ds(weights.columns(k, m), 128), :] for k, m in chips[4 * sub : 4 * sub + 4]],
+                axis=0)
             out = dot(block, hid_ref[...])
             for i in range(4):
-                part_ref[1, h, :, (j + i) * 128 : (j + i + 1) * 128] = (
+                part_ref[1, g, sub, :, i * 128 : (i + 1) * 128] = (
                     out[i * 128 : (i + 1) * 128].T.astype(BF16))
-        if h == 0:
-            across.first(1, part_ref.at[1], relay_ref, landed_ref)
-        else:
-            across.second(1, part_ref.at[1], relay_ref, landed_ref)
+        across.start_sum(1, g, part_ref.at[1], relay_ref, landed_ref)
     across.pass_on(1, 1, part_ref.at[1], relay_ref, landed_ref)
-    mixer = across.total(1, part_ref.at[1], landed_ref)
-    for j, (k, m) in enumerate(EARLY + LATE):
-        sum_ref[:, pl.ds(weights.columns(k, m), 128)] = mixer[:, j * 128 : (j + 1) * 128]
+    for g, chips in enumerate((EARLY, LATE)):
+        sums = across.total(1, g, part_ref.at[1], landed_ref)
+        for j, (k, m) in enumerate(chips):
+            piece = sums[j // 4][:, (j % 4) * 128 : (j % 4 + 1) * 128]
+            sum_ref[:, pl.ds(weights.columns(k, m), 128)] = piece
     merged = res_ref[...].astype(F32) + 0.5 * rms_scale(sum_ref[...], post_gain_ref[...])
-    out_ref[...] = merged.astype(BF16)
+    out_ref[...] = merged
     for copy in weights.started + across.started:
         copy.wait_send()
 
@@ -565,7 +600,7 @@
     held = [pltpu.VMEM(v.shape, v.dtype) for v in arrays[:14]]
     return pl.pallas_call(
         layer_kernel,
-        out_shape=jax.ShapeDtypeStruct((ROWS, D), BF16),
+        out_shape=jax.ShapeDtypeStruct((ROWS, D), F32),
         in_specs=[hbm] * len(arrays),
         out_specs=pl.BlockSpec(memory_space=pltpu.VMEM),
         scratch_shapes=[
@@ -581,14 +616,14 @@
             pltpu.VMEM((4, 32, 128), BF16),
             pltpu.VMEM((D, 2 * F), BF16),
             pltpu.VMEM((D, F), BF16),
-            pltpu.VMEM((2, 2, T, HALF), BF16),
-            pltpu.VMEM((2, 2, ROWS, HALF), BF16),
-            pltpu.VMEM((2, 2, 2, ROWS, HALF), BF16),
+            pltpu.VMEM((2, 2, 2, T, QUARTER), BF16),
+            pltpu.VMEM((2, 2, 2, ROWS, QUARTER), BF16),
+            pltpu.VMEM((2, 2, 2, 2, ROWS, QUARTER), BF16),
             pltpu.VMEM((T, D), BF16),
             pltpu.VMEM((F, T), BF16),
             pltpu.VMEM((ROWS, D), F32),
             dma((2, 8)), dma((2, 8)), dma((2, 4)), dma((2, 4)),
-            dma((2, 36)), dma((2, 36)), dma((3, 6)), dma((3, 6)), dma((15,)), dma((2 * TILES,)),
+            dma((2, 40)), dma((2, 40)), dma((3, 12)), dma((3, 12)), dma((15,)), dma((2,)),
         ],
         compiler_params=pltpu.CompilerParams(
             collective_id=0, has_side_effects=True, vmem_limit_bytes=66000000
@@ -609,7 +644,7 @@
         output_real.reshape(512, N), output_imaginary.reshape(512, N),
         mix_gain.reshape(1, D), pre_gain.reshape(1, D), post_gain.reshape(1, D),
     )
-    return layer(small + (out_weight, residual, gate_weight, up_weight, down_weight))
+    return layer(small + (out_weight, residual, gate_weight, up_weight, down_weight)).astype(BF16)
 
 
 def solution(mesh):

time: 76.2 us -> 70.6 us (0.927)
  the two profiles are of different devices: /device:TPU:4 before, /device:TPU:1 now
where the time goes in v3:
time: 70.6 us; the launch traced here: 69.4 us
  Pallas kernels  67.7 us (96%)
  other arithmetic  1.77 us (3%)
    pallas_call x1, Pallas kernels, layer(): pl.pallas_call(layer_kernel, out_shape=jax.ShapeDtypeStruct((ROWS, D), F3...  67.7 us
    convert_element_type x1, other arithmetic, shards(): layer(small + (out_weight, residual, gate_weight, up_weight, down_weight))  1.77 us

profile of v3, /device:TPU:1, one launch (start us, length us, event | category | flops | bytes accessed | tf_op | source)
XLA Modules:
  0.0 69.4 jit_solution(7554023187810938477)
XLA Ops:
  0.0 67.7 %layer.1 = f32[64,2048]{1,0:T(8,128)} custom-call(bf16[256,512]{1,0:T(8,128)(2,1)} %u_hbm.1, f32[32,256]{1,0:T(8,128)} %bitcast.17, f32[32,64]{1,0:T(8,128)} %pr_hbm.1, f32[32,64]{1,0:T(8,128)} %pi_hbm.1, f32[1,32]{1,0:T(1,128)} %bitcast.21, f32[512,64]{1,0:T(8,128)} %bitcast.13, f32[512,64]{1,0:T(8,128)} %bitcast.14, f32[512,64]{1,0:T(8,128)} %bitcast.15, ...), custom_call_target="tpu_custom_call" | custom-call | tf_op jit(solution)/shard_map/layer/pallas_call | solution.py:601
  67.7 1.8 %convert_element_type.3 = bf16[64,2048]{1,0:T(8,128)(2,1)} convert(f32[64,2048]{1,0:T(8,128)} %layer.1) | non-fusion elementwise | flops 131072 | bytes 786432 | tf_op jit(solution)/shard_map/convert_element_type | solution.py:647

commit v4 on v3

v4 whole, which is shorter than its diff:
```python
import functools

import jax
import jax.numpy as jnp
from jax import lax
from jax.experimental import pallas as pl
from jax.experimental.pallas import tpu as pltpu
from jax.sharding import PartitionSpec as P

EPSILON = 1e-06
EXACT = lax.Precision.HIGHEST
MESH = pl.DeviceIdType.MESH
F32 = jnp.float32
BF16 = jnp.bfloat16
T = 256
G = 32
N = 64
C = 16
GN = G * N
SEGS = 8
STEPS = T // SEGS
D = 2048
F = 1408
ROWS = 64
HALF = D // 2
TILES = F // 128


def dot(a, b, **kw):
    return jnp.dot(a, b, preferred_element_type=F32, **kw)


def dot_nt(a, b):
    return lax.dot_general(a, b, (((1,), (1,)), ((), ())), preferred_element_type=F32)


def iota(shape, dim):
    return lax.broadcasted_iota(jnp.int32, shape, dim)


def one_hot(mask, dtype):
    return jnp.where(mask, 1.0, 0.0).astype(dtype)


def cmul(ar, ai, br, bi):
    return ar * br - ai * bi, ar * bi + ai * br


def split(v):
    hi = v.astype(BF16)
    return hi, (v - hi.astype(F32)).astype(BF16)


def expm1(x):
    p = 1.0 / 40320.0
    for k in (5040.0, 720.0, 120.0, 24.0, 6.0, 2.0, 1.0):
        p = p * x + 1.0 / k
    return jnp.where(x > -0.5, p * x, jnp.exp(x) - 1.0)


def lanes_of(v, count):
    pair = jnp.concatenate([v, v], axis=1)
    return jnp.concatenate([pair] * (count // 128), axis=1)


def step_rows(pr, pi, sl, row):
    same = iota((G, G), 0) == iota((G, G), 1)
    column = jnp.sum(jnp.where(same, jnp.broadcast_to(sl, (G, G)), 0.0), axis=1, keepdims=True)
    pr, pi, step = row(lanes_of(pr, GN)), row(lanes_of(pi, GN)), jnp.exp(row(column))
    log_size = pr * step
    angle = pi * step
    cosine, sine = jnp.cos(angle), jnp.sin(angle)
    size = jnp.exp(log_size)
    half = jnp.sin(0.5 * angle)
    lift_r = expm1(log_size) * cosine - 2.0 * half * half
    lift_i = size * sine
    inv = 1.0 / (pr * pr + pi * pi)
    ratio_r = (lift_r * pr + lift_i * pi) * inv
    ratio_i = (lift_i * pr - lift_r * pi) * inv
    return size * cosine, size * sine, ratio_r, ratio_i


def thirds(v):
    hi = v.astype(BF16)
    rest = v - hi.astype(F32)
    mid = rest.astype(BF16)
    return jnp.concatenate([hi, mid, (rest - mid.astype(F32)).astype(BF16)], axis=0)


def scan_pass(base, e_ref, dr_ref, di_ref, init, store):
    ends = []
    width = GN // 4
    for lc in range(4):
        sl = slice(lc * width, (lc + 1) * width)
        br = jnp.broadcast_to(base[0][:, sl], (SEGS, width))
        bi = jnp.broadcast_to(base[1][:, sl], (SEGS, width))

        def body(i, st):
            sr, si, pe = st
            rows = pl.ds(pl.multiple_of(i * SEGS, SEGS), SEGS)
            e = e_ref[rows, sl]
            ar, ai = br * e, bi * e
            nr = ar * sr - ai * si + dr_ref[rows, sl]
            ni = ar * si + ai * sr + di_ref[rows, sl]
            if store:
                dr_ref[rows, sl] = nr
                di_ref[rows, sl] = ni
                return nr, ni, pe
            return nr, ni, pe * e

        st = (init[0][:, sl], init[1][:, sl], jnp.ones((SEGS, width), F32))
        ends.append(lax.fori_loop(0, STEPS, body, st, unroll=4))
    return [jnp.concatenate([p[k] for p in ends], axis=1) for k in range(3)]


def put_row(ref, slot, part, row):
    for k in range(16):
        ref[slot, part * 16 + k : part * 16 + k + 1, :] = row[:, k * 128 : (k + 1) * 128].astype(ref.dtype)


def to_block(row):
    return jnp.concatenate([row[:, k * 128 : (k + 1) * 128] for k in range(16)], axis=0)


def to_row(block):
    return jnp.concatenate([block[k : k + 1, :] for k in range(16)], axis=1)


def link(first, then):
    ar, ai, sr, si = first
    br, bi, tr, ti = then
    pr, pi = cmul(br, bi, ar, ai)
    ur, ui = cmul(br, bi, sr, si)
    return pr, pi, ur + tr, ui + ti


def choose(cond, a, b):
    return tuple(jnp.where(cond, x, y) for x, y in zip(a, b))


def rms_scale(values, gain):
    return values * lax.rsqrt(jnp.mean(values * values, axis=-1, keepdims=True) + EPSILON) * gain


class Gather:
    def __init__(self, refs, send, recv, sp):
        self.refs, self.send_sem, self.recv_sem = refs, send, recv
        core, y, z = sp % 2, (sp // 2) % 4, sp // 8
        self.core = core
        self.fm, self.sm = 1 + 3 * core, 4 - 3 * core
        f = y + core * (z - y)
        s = z + core * (y - z)
        self.fk = [f, (f + 3) % 4, (f + 1) % 4, (f + 2) % 4]
        self.sk = [s, (s + 3) % 4, (s + 1) % 4, (s + 2) % 4]
        self.f_next, self.f_prev = self.place(2, 0), self.place(1, 0)
        self.s_next, self.s_prev = self.place(0, 2), self.place(0, 1)
        self.partner = sp + 1 - 2 * core

    def place(self, k, m):
        return 2 * (self.fk[k] * self.fm + self.sk[m] * self.sm) + self.core

    def block(self, p, k, m, half=None):
        start = self.place(k, m) * ROWS
        return self.rows(p, start, half)

    def rows(self, p, start, half):
        if half is None:
            return self.refs[p].at[pl.ds(pl.multiple_of(start, ROWS), ROWS)]
        return self.refs[p].at[pl.ds(pl.multiple_of(start + half * 32, 32), 32)]

    def copy(self, p, sem, ref, dev):
        return pltpu.make_async_remote_copy(
            ref, ref, self.send_sem.at[p], self.recv_sem.at[p, sem],
            device_id={"sp": dev}, device_id_type=MESH)

    def send(self, p, sem, ref, dev):
        self.copy(p, sem, ref, dev).start()

    def arrive(self, p, sem, rows):
        self.copy(p, sem, self.refs[p].at[pl.ds(0, rows)], self.partner).wait_recv()

    def drain(self):
        for p in range(2):
            self.copy(p, 0, self.refs[p].at[pl.ds(0, 1984)], self.partner).wait_send()

    def hand(self, p, k, m):
        late = p == 1 and (k == 3 or m == 3)
        self.send(p, 1 if late else 11, self.block(p, k, m), self.partner)

    def handed(self, p, sem, count):
        self.arrive(p, sem, count * ROWS)

    def own_along(self, p, turn, half):
        own = self.block(p, 0, 0, half)
        nexts, prevs = (self.f_next, self.s_next), (self.f_prev, self.s_prev)
        for side, (f_dev, s_dev) in enumerate((nexts, prevs)):
            f_sem = 0 if p == 1 or (half == 0 and side == 0) else 1
            self.send(p, f_sem + turn * (3 - f_sem), own, f_dev + turn * (s_dev - f_dev))

    def beyond_f(self, p):
        self.arrive(p, 0, 128)
        self.send(p, 2, self.block(p, 1, 0, 0), self.f_next)
        self.send(p, 2, self.block(p, 2, 0, 1), self.f_prev)

    def beyond_f_next(self):
        self.arrive(0, 0, 32)
        self.send(0, 2, self.block(0, 1, 0, 0), self.f_next)

    def beyond_f_prev(self):
        self.arrive(0, 1, 96)
        self.send(0, 2, self.block(0, 2, 0, 1), self.f_prev)

    def opposite_f(self, p):
        self.arrive(p, 2, 64)

    def beyond_s_own(self):
        self.beyond_s(0, 0)

    def along_s(self, p, k):
        ref = self.block(p, k, 0)
        self.send(p, 3 + k, ref, self.s_next)
        self.send(p, 3 + k, ref, self.s_prev)
        self.hand(p, k, 0)

    def beyond_s(self, p, k):
        self.arrive(p, 3 + k, 128)
        self.send(p, 7 + k, self.block(p, k, 1, 0), self.s_next)
        self.send(p, 7 + k, self.block(p, k, 2, 1), self.s_prev)
        self.hand(p, k, 1)
        self.hand(p, k, 2)

    def opposite_s(self, p, k):
        self.arrive(p, 7 + k, 64)
        self.hand(p, k, 3)

    def columns(self, k, m):
        return pl.multiple_of((self.fk[k] * self.fm + self.sk[m] * self.sm) * 128, 128)


class Across:
    def __init__(self, x, send, recv):
        self.x, self.send_sem, self.recv_sem = x, send, recv
        self.next, self.prev, self.far = (x + 1) % 4, (x + 3) % 4, (x + 2) % 4

    def copy(self, phase, sem, src, dst, dev):
        return pltpu.make_async_remote_copy(
            src, dst, self.send_sem.at[phase], self.recv_sem.at[phase, sem],
            device_id={"tp": dev}, device_id_type=MESH)

    def send(self, phase, sem, src, dst, dev):
        self.copy(phase, sem, src, dst, dev).start()

    def arrive(self, phase, sem, ref):
        self.copy(phase, sem, ref, ref, self.next).wait_recv()

    def drain(self, phase, ref):
        self.copy(phase, 0, ref, ref, self.next).wait_send()

    def rows(self, x, half=None):
        if half is None:
            return pl.ds(pl.multiple_of(x * ROWS, ROWS), ROWS)
        return pl.ds(pl.multiple_of(x * ROWS + half * 32, 32), 32)

    def start_relay(self, phase, g, part, relay):
        self.send(phase, g, part.at[g, 0, self.rows(self.far)], relay.at[phase, g, 0], self.next)
        self.send(phase, g, part.at[g, 1, self.rows(self.far)], relay.at[phase, g, 1], self.prev)

    def start_own(self, phase, g, part, landed):
        self.send(
            phase, 2 + g, part.at[g, 1, self.rows(self.next)], landed.at[phase, g, 0, 1], self.next)
        self.send(
            phase, 2 + g, part.at[g, 0, self.rows(self.prev)], landed.at[phase, g, 1, 0], self.prev)

    def pass_on(self, phase, g, part, relay, landed):
        self.arrive(phase, g, relay.at[phase, g])
        for side, dev in ((0, self.next), (1, self.prev)):
            total = relay[phase, g, side].astype(F32) + part[g, side, self.rows(dev)].astype(F32)
            relay[phase, g, side] = total.astype(BF16)
            self.send(phase, 2 + g, relay.at[phase, g, side], landed.at[phase, g, side, side], dev)

    def total(self, phase, g, part, landed):
        self.arrive(phase, 2 + g, landed.at[phase, g])
        return [
            part[g, sub, self.rows(self.x)].astype(F32)
            + landed[phase, g, 0, sub].astype(F32)
            + landed[phase, g, 1, sub].astype(F32)
            for sub in range(2)
        ]

    def share(self, ref):
        top, bottom = (ref.at[self.rows(self.x, half)] for half in range(2))
        self.send(2, 0, top, top, self.next)
        self.send(2, 1, bottom, bottom, self.prev)
        self.send(2, 2, bottom, bottom, self.next)
        self.send(2, 2, top, top, self.prev)

    def share_on(self, ref):
        top, bottom = ref.at[self.rows(self.prev, 0)], ref.at[self.rows(self.next, 1)]
        self.arrive(2, 0, top)
        self.send(2, 2, top, top, self.next)
        self.arrive(2, 1, bottom)
        self.send(2, 2, bottom, bottom, self.prev)

    def shared(self, ref):
        self.arrive(2, 2, ref.at[pl.ds(0, 128)])


QUARTER = D // 4
EARLY = [(0, 0), (1, 0), (2, 0), (0, 1), (0, 2), (1, 1), (1, 2), (2, 1)]
LATE = [(2, 2), (3, 0), (3, 1), (3, 2), (0, 3), (1, 3), (2, 3), (3, 3)]


def layer_kernel(
    u_hbm, a_hbm, pr_hbm, pi_hbm, sl_hbm, bre_hbm, bim_hbm, cre_hbm, cim_hbm,
    mix_gain_hbm, pre_gain_hbm, post_gain_hbm, wo_hbm, res_hbm, gate_hbm, up_hbm, down_hbm,
    out_ref,
    u_ref, a_ref, poles_ref, sl_ref, maps_ref, gains_ref, wo_ref, res_ref,
    e_ref, dr_ref, di_ref, act_ref, read_ref, ea_ref, eb_ref, ra_ref, rb_ref, gu_ref, dn_ref,
    part_ref, relay_ref, landed_ref, rows_ref, hid_ref, sum_ref,
    cs, cq, ws, wq, xs, xq, ls,
):
    sp = lax.axis_index("sp")
    tp = lax.axis_index("tp")
    q = sp % 8
    z = sp // 8
    peers_a = [z * 8 + (q + d) % 8 for d in range(1, 8)]
    peers_b = [((z + d) % 4) * 8 + q for d in range(1, 4)]
    weights = Gather((gu_ref, dn_ref), ws, wq, sp)
    across = Across(tp, xs, xq)
    own = pl.ds(pl.multiple_of(sp * ROWS, ROWS), ROWS)
    for side, hbm in enumerate((gate_hbm, up_hbm)):
        pltpu.make_async_copy(hbm, gu_ref.at[own, pl.ds(side * F, F)], ls.at[0]).start()
    barrier = pltpu.get_barrier_semaphore()
    for peer in peers_a + peers_b:
        pl.semaphore_signal(barrier, inc=1, device_id={"sp": peer}, device_id_type=MESH)
    for peer in (across.next, across.prev):
        pl.semaphore_signal(barrier, inc=1, device_id={"tp": peer}, device_id_type=MESH)
    pairs = (
        (a_hbm, a_ref, 1), (pr_hbm, poles_ref.at[0], 2), (pi_hbm, poles_ref.at[1], 2),
        (sl_hbm, sl_ref, 3), (u_hbm, u_ref, 4),
        (bre_hbm, maps_ref.at[0], 5), (bim_hbm, maps_ref.at[1], 5),
        (cre_hbm, maps_ref.at[2], 5), (cim_hbm, maps_ref.at[3], 5),
        (wo_hbm, wo_ref, 6), (res_hbm, res_ref, 7), (mix_gain_hbm, gains_ref.at[0], 8),
        (pre_gain_hbm, gains_ref.at[1], 8), (post_gain_hbm, gains_ref.at[2], 8),
        (down_hbm, dn_ref.at[own], 9),
    )
    for src, dst, sem in pairs:
        pltpu.make_async_copy(src, dst, ls.at[sem]).start()

    def loaded(ref, sem):
        pltpu.make_async_copy(ref, ref, ls.at[sem]).wait()

    mine = iota((G, GN), 1) // N == iota((G, GN), 0)

    def row(v):
        return jnp.sum(jnp.where(mine, v, 0.0), axis=0, keepdims=True)

    loaded(a_ref, 1)
    put_row(ea_ref, 0, 0, jnp.exp(row(jnp.sum(a_ref[...], axis=1, keepdims=True))))
    loaded(gu_ref.at[own], 0)
    pl.semaphore_wait(barrier, 12)

    def to_all(ref, peers, sem):
        for d, peer in enumerate(peers, 1):
            pltpu.make_async_remote_copy(
                ref.at[0], ref.at[d], cs.at[sem], cq.at[sem],
                device_id={"sp": peer}, device_id_type=MESH).start()

    def from_all(ref, peers, sem):
        others = ref.at[pl.ds(1, len(peers))]
        pltpu.make_async_remote_copy(
            others, others, cs.at[sem], cq.at[sem],
            device_id={"sp": peers[0]}, device_id_type=MESH).wait()

    to_all(ea_ref, peers_a, 0)
    weights.own_along(0, weights.core, 0)
    weights.own_along(0, 1 - weights.core, 0)
    weights.own_along(0, 1 - weights.core, 1)
    weights.hand(0, 0, 0)
    loaded(poles_ref, 2)
    loaded(sl_ref, 3)

    base_r, base_i, ratio_r, ratio_i = step_rows(poles_ref[0], poles_ref[1], sl_ref[...], row)

    perm = iota((T, T), 0) == (iota((T, T), 1) % SEGS) * STEPS + iota((T, T), 1) // SEGS
    order = iota((T, T), 1) == (iota((T, T), 0) % SEGS) * STEPS + iota((T, T), 0) // SEGS
    e_small = dot(thirds(jnp.exp(a_ref[...])), one_hot(perm, BF16)).astype(BF16)
    groups = one_hot(mine, BF16)
    e_ref[...] = lax.dot_general(
        e_small, jnp.concatenate([groups] * 3, axis=0), (((0,), (0,)), ((), ())),
        preferred_element_type=F32)
    loaded(u_ref, 4)
    loaded(maps_ref, 5)
    u = dot(one_hot(order, BF16), u_ref[...]).astype(BF16)
    inside = iota((256, 1024), 0) // C == iota((256, 1024), 1) // N

    def spread(v):
        return jnp.where(inside, lanes_of(v, 1024), 0.0).astype(BF16)

    for h in range(2):
        gn = slice(h * 1024, (h + 1) * 1024)
        ch = slice(h * 256, (h + 1) * 256)
        raw_r = dot(u[:, ch], spread(maps_ref[0, ch, :]))
        raw_i = dot(u[:, ch], spread(maps_ref[1, ch, :]))
        rr, ri = ratio_r[:, gn], ratio_i[:, gn]
        dr_ref[:, gn] = rr * raw_r - ri * raw_i
        di_ref[:, gn] = rr * raw_i + ri * raw_r

    zero = jnp.zeros((SEGS, GN), F32)
    end_r, end_i, pe = scan_pass((base_r, base_i), e_ref, dr_ref, di_ref, (zero, zero), False)
    wr, wi = base_r, base_i
    for _ in range(5):
        wr, wi = cmul(wr, wi, wr, wi)
    seg_r, seg_i = wr * pe, wi * pe
    one_row = jnp.ones((1, GN), F32)
    no_row = jnp.zeros((1, GN), F32)
    total = (one_row, no_row, no_row, no_row)
    before = []
    for j in range(SEGS):
        before.append(total)
        total = link(total, (seg_r[j : j + 1], seg_i[j : j + 1], end_r[j : j + 1], end_i[j : j + 1]))
    put_row(ra_ref, 0, 0, total[2])
    put_row(ra_ref, 0, 1, total[3])

    to_all(ra_ref, peers_a, 1)
    weights.own_along(0, weights.core, 1)
    loaded(dn_ref.at[own], 9)
    weights.own_along(1, weights.core, None)
    weights.hand(1, 0, 0)
    for h in range(2):
        ch = slice(h * 256, (h + 1) * 256)
        read_ref[h, 0] = spread(maps_ref[2, ch, :])
        read_ref[h, 1] = spread(-maps_ref[3, ch, :])
    w_r, w_i = to_block(wr), to_block(wi)
    for _ in range(3):
        w_r, w_i = cmul(w_r, w_i, w_r, w_i)
    v_r, v_i = w_r, w_i
    for _ in range(3):
        v_r, v_i = cmul(v_r, v_i, v_r, v_i)
    from_all(ea_ref, peers_a, 0)
    eb = ea_ref[0]
    for d in range(1, 8):
        eb = eb * ea_ref[d]
    eb_ref[0] = eb
    to_all(eb_ref, peers_b, 2)
    from_all(ra_ref, peers_a, 1)
    unit = jnp.ones((16, 128), F32)
    null = jnp.zeros((16, 128), F32)

    def stretch(e, pr, pi, ref, slot):
        block = ref[slot].astype(F32)
        decay = e[slot]
        return pr * decay, pi * decay, block[:16], block[16:]

    run = (unit, null, null, null)
    pre_a = run
    for k in range(8):
        pre_a = choose(q == k, run, pre_a)
        run = link(run, stretch(ea_ref, w_r, w_i, ra_ref, (q - k + 8) % 8))
    rb_ref[0, :16] = run[2].astype(BF16)
    rb_ref[0, 16:] = run[3].astype(BF16)
    to_all(rb_ref, peers_b, 3)
    weights.own_along(1, 1 - weights.core, None)
    weights.beyond_f_next()
    weights.beyond_f_prev()
    weights.along_s(0, 1)
    weights.along_s(0, 2)
    from_all(eb_ref, peers_b, 2)
    from_all(rb_ref, peers_b, 3)
    run = (unit, null, null, null)
    pre_b = run
    for k in range(4):
        pre_b = choose(z == k, run, pre_b)
        run = link(run, stretch(eb_ref, v_r, v_i, rb_ref, (z - k + 4) % 4))
    carry = link(pre_b, pre_a)
    cr, ci = to_row(carry[2]), to_row(carry[3])
    starts = []
    for k in range(SEGS):
        pr, pi, sr, si = before[k]
        tr, ti = cmul(pr, pi, cr, ci)
        starts.append((tr + sr, ti + si))
    init = [jnp.concatenate([s[k] for s in starts], axis=0) for k in range(2)]
    scan_pass((base_r, base_i), e_ref, dr_ref, di_ref, init, True)

    for h in range(2):
        gn = slice(h * 1024, (h + 1) * 1024)
        y = dot_nt(dr_ref[:, gn].astype(BF16), read_ref[h, 0])
        y = y + dot_nt(di_ref[:, gn].astype(BF16), read_ref[h, 1])
        act_ref[:, h * 256 : (h + 1) * 256] = jax.nn.gelu(y).astype(BF16)
    act = dot(one_hot(perm, BF16), act_ref[...]).astype(BF16)
    loaded(wo_ref, 6)
    for g in range(2):
        out = dot(act, wo_ref[:, g * HALF : (g + 1) * HALF]).astype(BF16)
        part_ref[0, g, 0] = out[:, :QUARTER]
        part_ref[0, g, 1] = out[:, QUARTER:]
        across.start_relay(0, g, part_ref.at[0], relay_ref)
        across.start_own(0, g, part_ref.at[0], landed_ref)
    weights.beyond_s_own()
    across.pass_on(0, 0, part_ref.at[0], relay_ref, landed_ref)
    weights.opposite_f(0)
    weights.along_s(0, 3)
    across.pass_on(0, 1, part_ref.at[0], relay_ref, landed_ref)
    weights.beyond_s(0, 1)
    weights.beyond_f(1)
    mixed = jnp.concatenate(
        across.total(0, 0, part_ref.at[0], landed_ref)
        + across.total(0, 1, part_ref.at[0], landed_ref), axis=1)
    loaded(res_ref, 7)
    loaded(gains_ref, 8)
    middle = (res_ref[...].astype(F32) + rms_scale(mixed, gains_ref[0])).astype(BF16)
    res_ref[...] = middle
    normed = rms_scale(middle.astype(F32), gains_ref[1]).astype(BF16)
    rows_ref[across.rows(tp), :] = normed
    across.share(rows_ref)
    weights.beyond_s(0, 2)
    across.share_on(rows_ref)
    weights.beyond_s(0, 3)
    weights.along_s(1, 1)
    weights.along_s(1, 2)
    weights.opposite_f(1)
    weights.along_s(1, 3)
    weights.beyond_s(1, 0)
    across.shared(rows_ref)
    for k in range(4):
        weights.opposite_s(0, k)
    weights.handed(0, 11, 16)
    def hidden_tile(gate, up, first):
        hidden = gate / (1.0 + jnp.exp(-gate)) * up
        hid_ref[first : first + gate.shape[1], :] = hidden.T.astype(BF16)

    for first in range(0, F - 128, 256):
        tile = [gu_ref[:, side * F + first : side * F + first + 256] for side in range(2)]
        hidden_tile(dot(rows_ref[...], tile[0]), dot(rows_ref[...], tile[1]), first)
        if first in (256, 1024):
            weights.beyond_s(1, 1 if first == 256 else 2)
    both = dot(rows_ref[...], jnp.concatenate([gu_ref[:, F - 128 : F], gu_ref[:, 2 * F - 128 :]], axis=1))
    hidden_tile(both[:, :128], both[:, 128:], F - 128)

    weights.beyond_s(1, 3)
    weights.handed(1, 11, 9)
    for g, chips in enumerate((EARLY, LATE)):
        if g == 1:
            for i in range(4):
                weights.opposite_s(1, i)
            weights.handed(1, 1, 7)
        for sub in range(2):
            block = jnp.concatenate(
                [dn_ref[pl.ds(weights.columns(k, m), 128), :] for k, m in chips[4 * sub : 4 * sub + 4]],
                axis=0)
            out = dot(block, hid_ref[...])
            for i in range(4):
                part_ref[1, g, sub, :, i * 128 : (i + 1) * 128] = (
                    out[i * 128 : (i + 1) * 128].T.astype(BF16))
        across.start_relay(1, g, part_ref.at[1], relay_ref)
        if g == 1:
            across.pass_on(1, 0, part_ref.at[1], relay_ref, landed_ref)
        across.start_own(1, g, part_ref.at[1], landed_ref)
    across.pass_on(1, 1, part_ref.at[1], relay_ref, landed_ref)
    for g, chips in enumerate((EARLY, LATE)):
        sums = across.total(1, g, part_ref.at[1], landed_ref)
        for j, (k, m) in enumerate(chips):
            piece = sums[j // 4][:, (j % 4) * 128 : (j % 4 + 1) * 128]
            sum_ref[:, pl.ds(weights.columns(k, m), 128)] = piece
    merged = res_ref[...].astype(F32) + 0.5 * rms_scale(sum_ref[...], gains_ref[2])
    out_ref[...] = merged.astype(BF16)
    weights.drain()
    across.drain(0, part_ref.at[0, :, :, pl.ds(0, 192)])
    across.drain(1, part_ref.at[1, :, :, pl.ds(0, 192)])
    across.drain(2, rows_ref.at[pl.ds(0, 192)])


def layer(arrays):
    hbm = pl.BlockSpec(memory_space=pl.ANY)
    dma = pltpu.SemaphoreType.DMA
    return pl.pallas_call(
        layer_kernel,
        out_shape=jax.ShapeDtypeStruct((ROWS, D), BF16),
        in_specs=[hbm] * len(arrays),
        out_specs=pl.BlockSpec(memory_space=pltpu.VMEM),
        scratch_shapes=[
            pltpu.VMEM((T, 512), BF16),
            pltpu.VMEM((G, T), F32),
            pltpu.VMEM((2, G, N), F32),
            pltpu.VMEM((1, G), F32),
            pltpu.VMEM((4, 512, N), F32),
            pltpu.VMEM((3, 1, D), F32),
            pltpu.VMEM((512, D), BF16),
            pltpu.VMEM((ROWS, D), BF16),
            pltpu.VMEM((T, GN), F32),
            pltpu.VMEM((T, GN), F32),
            pltpu.VMEM((T, GN), F32),
            pltpu.VMEM((T, 512), BF16),
            pltpu.VMEM((2, 2, 256, 1024), BF16),
            pltpu.VMEM((8, 16, 128), F32),
            pltpu.VMEM((4, 16, 128), F32),
            pltpu.VMEM((8, 32, 128), BF16),
            pltpu.VMEM((4, 32, 128), BF16),
            pltpu.VMEM((D, 2 * F), BF16),
            pltpu.VMEM((D, F), BF16),
            pltpu.VMEM((2, 2, 2, T, QUARTER), BF16),
            pltpu.VMEM((2, 2, 2, ROWS, QUARTER), BF16),
            pltpu.VMEM((2, 2, 2, 2, ROWS, QUARTER), BF16),
            pltpu.VMEM((T, D), BF16),
            pltpu.VMEM((F, T), BF16),
            pltpu.VMEM((ROWS, D), F32),
            dma((4,)), dma((4,)), dma((2,)), dma((2, 12)), dma((3,)), dma((3, 4)), dma((10,)),
        ],
        compiler_params=pltpu.CompilerParams(
            collective_id=0, has_side_effects=True, vmem_limit_bytes=66000000
        ),
        name="layer",
    )(*arrays)


def shards(
    residual, ssm_input, pole_real, pole_imaginary, step_log, input_real, entry_map_quadrature,
    output_real, output_imaginary, added_log_decay, out_weight, mix_gain, gate_weight, up_weight,
    down_weight, pre_gain, post_gain,
):
    small = (
        ssm_input, added_log_decay.T, pole_real, pole_imaginary, step_log.reshape(1, G),
        input_real.transpose(0, 2, 1).reshape(512, N),
        entry_map_quadrature.transpose(0, 2, 1).reshape(512, N),
        output_real.reshape(512, N), output_imaginary.reshape(512, N),
        mix_gain.reshape(1, D), pre_gain.reshape(1, D), post_gain.reshape(1, D),
    )
    return layer(small + (out_weight, residual, gate_weight, up_weight, down_weight))


def solution(mesh):
    return jax.shard_map(
        shards,
        mesh=mesh,
        in_specs=(
            P(("sp", "tp"), None), P("sp", "tp"), P("tp", None), P("tp", None), P("tp"),
            P("tp", None, None), P("tp", None, None), P("tp", None, None), P("tp", None, None),
            P("sp", "tp"), P("tp", None), P(), P("sp", "tp"), P("sp", "tp"), P("sp", "tp"),
            P(), P(),
        ),
        out_specs=P(("sp", "tp"), None),
        check_vma=False,
    )
```

time: 70.6 us -> 68.6 us (0.972); the launches traced: 69.4 us -> 68.5 us
  other arithmetic: 1.77 us -> 0 us
  local copies, waits for them, and re-layouts: 0 us -> 1.67 us
  Pallas kernels: 67.7 us -> 66.8 us
    convert_element_type x1 -> x0, other arithmetic: 1.77 us -> none  [shards(): layer(small + (out_weight, residual, gate_weight, up_weight, down_weight))]
    unnamed x0 -> x1, local copies, waits for them, and re-layouts: none -> 1.67 us
    pallas_call x1, Pallas kernels: 67.7 us -> 66.8 us  [layer(): pl.pallas_call(layer_kernel, out_shape=jax.ShapeDtypeStruct((ROWS, D), BF...]
where the time goes in v4:
time: 68.6 us; the launch traced here: 68.5 us
  Pallas kernels  66.8 us (97%)
  local copies, waits for them, and re-layouts  1.67 us (2%)
    pallas_call x1, Pallas kernels, layer(): pl.pallas_call(layer_kernel, out_shape=jax.ShapeDtypeStruct((ROWS, D), BF...  66.8 us
    unnamed x1, local copies, waits for them, and re-layouts  1.67 us

profile of v4, /device:TPU:1, one launch (start us, length us, event | category | flops | bytes accessed | tf_op | source)
XLA Modules:
  0.0 68.5 jit_solution(1820920578834167325)
XLA Ops:
  0.0 66.8 %layer.1 = bf16[64,2048]{1,0:T(8,128)(2,1)} custom-call(bf16[256,512]{1,0:T(8,128)(2,1)} %u_hbm.1, f32[32,256]{1,0:T(8,128)} %bitcast.17, f32[32,64]{1,0:T(8,128)} %pr_hbm.1, f32[32,64]{1,0:T(8,128)} %pi_hbm.1, f32[1,32]{1,0:T(1,128)} %bitcast.21, f32[512,64]{1,0:T(8,128)} %bitcast.13, f32[512,64]{1,0:T(8,128)} %bitcast.14, f32[512,64]{1,0:T(8,128)} %bitcast.15, ...), custom_call_target="tpu_custom_call" | custom-call | tf_op jit(solution)/shard_map/layer/pallas_call | solution.py:575
  66.8 1.7 %copy.19 = bf16[64,2048]{1,0:T(8,128)(2,1)} copy(bf16[64,2048]{1,0:T(8,128)(2,1)} %layer.1) | data formatting | bytes 524288

commit v5 on v4

--- a/solution.py
+++ b/solution.py
@@ -142,6 +142,15 @@
     return values * lax.rsqrt(jnp.mean(values * values, axis=-1, keepdims=True) + EPSILON) * gain
 
 
+CHIPS = (
+    ((0, 0), (0, 1), (1, 0), (0, 2)),
+    ((2, 0), (1, 1), (1, 2), (2, 1)),
+    ((2, 2), (3, 0), (0, 3), (1, 3)),
+    ((3, 1), (2, 3), (3, 2), (3, 3)),
+)
+GROUP_SEMS = (11, 1, 12, 13)
+
+
 class Gather:
     def __init__(self, refs, send, recv, sp):
         self.refs, self.send_sem, self.recv_sem = refs, send, recv
@@ -184,8 +193,11 @@
             self.copy(p, 0, self.refs[p].at[pl.ds(0, 1984)], self.partner).wait_send()
 
     def hand(self, p, k, m):
-        late = p == 1 and (k == 3 or m == 3)
-        self.send(p, 1 if late else 11, self.block(p, k, m), self.partner)
+        group = next(g for g in range(4) if (m, k) in CHIPS[g])
+        self.send(p, GROUP_SEMS[group] if p == 1 else 11, self.block(p, k, m), self.partner)
+
+    def handed_group(self, g):
+        self.arrive(1, GROUP_SEMS[g], 4 * ROWS)
 
     def handed(self, p, sem, count):
         self.arrive(p, sem, count * ROWS)
@@ -244,7 +256,7 @@
 
     def copy(self, phase, sem, src, dst, dev):
         return pltpu.make_async_remote_copy(
-            src, dst, self.send_sem.at[phase], self.recv_sem.at[phase, sem],
+            src, dst, self.send_sem.at[phase], self.recv_sem.at[(0, 4, 12)[phase] + sem],
             device_id={"tp": dev}, device_id_type=MESH)
 
     def send(self, phase, sem, src, dst, dev):
@@ -262,28 +274,28 @@
         return pl.ds(pl.multiple_of(x * ROWS + half * 32, 32), 32)
 
     def start_relay(self, phase, g, part, relay):
-        self.send(phase, g, part.at[g, 0, self.rows(self.far)], relay.at[phase, g, 0], self.next)
-        self.send(phase, g, part.at[g, 1, self.rows(self.far)], relay.at[phase, g, 1], self.prev)
+        self.send(phase, g, part.at[g, 0, self.rows(self.far)], relay.at[g, 0], self.next)
+        self.send(phase, g, part.at[g, 1, self.rows(self.far)], relay.at[g, 1], self.prev)
 
     def start_own(self, phase, g, part, landed):
         self.send(
-            phase, 2 + g, part.at[g, 1, self.rows(self.next)], landed.at[phase, g, 0, 1], self.next)
+            phase, part.shape[0] + g, part.at[g, 1, self.rows(self.next)], landed.at[g, 0, 1], self.next)
         self.send(
-            phase, 2 + g, part.at[g, 0, self.rows(self.prev)], landed.at[phase, g, 1, 0], self.prev)
+            phase, part.shape[0] + g, part.at[g, 0, self.rows(self.prev)], landed.at[g, 1, 0], self.prev)
 
     def pass_on(self, phase, g, part, relay, landed):
-        self.arrive(phase, g, relay.at[phase, g])
+        self.arrive(phase, g, relay.at[g])
         for side, dev in ((0, self.next), (1, self.prev)):
-            total = relay[phase, g, side].astype(F32) + part[g, side, self.rows(dev)].astype(F32)
-            relay[phase, g, side] = total.astype(BF16)
-            self.send(phase, 2 + g, relay.at[phase, g, side], landed.at[phase, g, side, side], dev)
+            total = relay[g, side].astype(F32) + part[g, side, self.rows(dev)].astype(F32)
+            relay[g, side] = total.astype(BF16)
+            self.send(phase, part.shape[0] + g, relay.at[g, side], landed.at[g, side, side], dev)
 
     def total(self, phase, g, part, landed):
-        self.arrive(phase, 2 + g, landed.at[phase, g])
+        self.arrive(phase, part.shape[0] + g, landed.at[g])
         return [
             part[g, sub, self.rows(self.x)].astype(F32)
-            + landed[phase, g, 0, sub].astype(F32)
-            + landed[phase, g, 1, sub].astype(F32)
+            + landed[g, 0, sub].astype(F32)
+            + landed[g, 1, sub].astype(F32)
             for sub in range(2)
         ]
 
@@ -306,17 +318,13 @@
 
 
 QUARTER = D // 4
-EARLY = [(0, 0), (1, 0), (2, 0), (0, 1), (0, 2), (1, 1), (1, 2), (2, 1)]
-LATE = [(2, 2), (3, 0), (3, 1), (3, 2), (0, 3), (1, 3), (2, 3), (3, 3)]
-
-
 def layer_kernel(
     u_hbm, a_hbm, pr_hbm, pi_hbm, sl_hbm, bre_hbm, bim_hbm, cre_hbm, cim_hbm,
     mix_gain_hbm, pre_gain_hbm, post_gain_hbm, wo_hbm, res_hbm, gate_hbm, up_hbm, down_hbm,
     out_ref,
     u_ref, a_ref, poles_ref, sl_ref, maps_ref, gains_ref, wo_ref, res_ref,
     e_ref, dr_ref, di_ref, act_ref, read_ref, ea_ref, eb_ref, ra_ref, rb_ref, gu_ref, dn_ref,
-    part_ref, relay_ref, landed_ref, rows_ref, hid_ref, sum_ref,
+    mix_part, out_part, mix_relay, out_relay, mix_landed, out_landed, rows_ref, hid_ref, sum_ref,
     cs, cq, ws, wq, xs, xq, ls,
 ):
     sp = lax.axis_index("sp")
@@ -491,20 +499,20 @@
     loaded(wo_ref, 6)
     for g in range(2):
         out = dot(act, wo_ref[:, g * HALF : (g + 1) * HALF]).astype(BF16)
-        part_ref[0, g, 0] = out[:, :QUARTER]
-        part_ref[0, g, 1] = out[:, QUARTER:]
-        across.start_relay(0, g, part_ref.at[0], relay_ref)
-        across.start_own(0, g, part_ref.at[0], landed_ref)
+        mix_part[g, 0] = out[:, :QUARTER]
+        mix_part[g, 1] = out[:, QUARTER:]
+        across.start_relay(0, g, mix_part, mix_relay)
+        across.start_own(0, g, mix_part, mix_landed)
     weights.beyond_s_own()
-    across.pass_on(0, 0, part_ref.at[0], relay_ref, landed_ref)
+    across.pass_on(0, 0, mix_part, mix_relay, mix_landed)
     weights.opposite_f(0)
     weights.along_s(0, 3)
-    across.pass_on(0, 1, part_ref.at[0], relay_ref, landed_ref)
+    across.pass_on(0, 1, mix_part, mix_relay, mix_landed)
     weights.beyond_s(0, 1)
     weights.beyond_f(1)
     mixed = jnp.concatenate(
-        across.total(0, 0, part_ref.at[0], landed_ref)
-        + across.total(0, 1, part_ref.at[0], landed_ref), axis=1)
+        across.total(0, 0, mix_part, mix_landed)
+        + across.total(0, 1, mix_part, mix_landed), axis=1)
     loaded(res_ref, 7)
     loaded(gains_ref, 8)
     middle = (res_ref[...].astype(F32) + rms_scale(mixed, gains_ref[0])).astype(BF16)
@@ -536,36 +544,40 @@
     both = dot(rows_ref[...], jnp.concatenate([gu_ref[:, F - 128 : F], gu_ref[:, 2 * F - 128 :]], axis=1))
     hidden_tile(both[:, :128], both[:, 128:], F - 128)
 
+    def down(g):
+        weights.handed_group(g)
+        block = jnp.concatenate(
+            [dn_ref[pl.ds(weights.columns(k, m), 128), :] for k, m in CHIPS[g]], axis=0)
+        out = dot(block, hid_ref[...])
+        for i in range(4):
+            out_part[g, i // 2, :, (i % 2) * 128 : (i % 2 + 1) * 128] = (
+                out[i * 128 : (i + 1) * 128].T.astype(BF16))
+        across.start_relay(1, g, out_part, out_relay)
+        across.start_own(1, g, out_part, out_landed)
+
+    down(0)
     weights.beyond_s(1, 3)
-    weights.handed(1, 11, 9)
-    for g, chips in enumerate((EARLY, LATE)):
-        if g == 1:
-            for i in range(4):
-                weights.opposite_s(1, i)
-            weights.handed(1, 1, 7)
-        for sub in range(2):
-            block = jnp.concatenate(
-                [dn_ref[pl.ds(weights.columns(k, m), 128), :] for k, m in chips[4 * sub : 4 * sub + 4]],
-                axis=0)
-            out = dot(block, hid_ref[...])
-            for i in range(4):
-                part_ref[1, g, sub, :, i * 128 : (i + 1) * 128] = (
-                    out[i * 128 : (i + 1) * 128].T.astype(BF16))
-        across.start_relay(1, g, part_ref.at[1], relay_ref)
-        if g == 1:
-            across.pass_on(1, 0, part_ref.at[1], relay_ref, landed_ref)
-        across.start_own(1, g, part_ref.at[1], landed_ref)
-    across.pass_on(1, 1, part_ref.at[1], relay_ref, landed_ref)
-    for g, chips in enumerate((EARLY, LATE)):
-        sums = across.total(1, g, part_ref.at[1], landed_ref)
+    down(1)
+    weights.opposite_s(1, 0)
+    weights.opposite_s(1, 1)
+    down(2)
+    weights.opposite_s(1, 2)
+    weights.opposite_s(1, 3)
+    across.pass_on(1, 0, out_part, out_relay, out_landed)
+    down(3)
+    across.pass_on(1, 1, out_part, out_relay, out_landed)
+    across.pass_on(1, 2, out_part, out_relay, out_landed)
+    across.pass_on(1, 3, out_part, out_relay, out_landed)
+    for g, chips in enumerate(CHIPS):
+        sums = across.total(1, g, out_part, out_landed)
         for j, (k, m) in enumerate(chips):
-            piece = sums[j // 4][:, (j % 4) * 128 : (j % 4 + 1) * 128]
+            piece = sums[j // 2][:, (j % 2) * 128 : (j % 2 + 1) * 128]
             sum_ref[:, pl.ds(weights.columns(k, m), 128)] = piece
     merged = res_ref[...].astype(F32) + 0.5 * rms_scale(sum_ref[...], gains_ref[2])
     out_ref[...] = merged.astype(BF16)
     weights.drain()
-    across.drain(0, part_ref.at[0, :, :, pl.ds(0, 192)])
-    across.drain(1, part_ref.at[1, :, :, pl.ds(0, 192)])
+    across.drain(0, mix_part.at[:, :, pl.ds(0, 192)])
+    across.drain(1, out_part.at[:, :, pl.ds(0, 192)])
     across.drain(2, rows_ref.at[pl.ds(0, 192)])
 
 
@@ -597,13 +609,16 @@
             pltpu.VMEM((4, 32, 128), BF16),
             pltpu.VMEM((D, 2 * F), BF16),
             pltpu.VMEM((D, F), BF16),
-            pltpu.VMEM((2, 2, 2, T, QUARTER), BF16),
+            pltpu.VMEM((2, 2, T, QUARTER), BF16),
+            pltpu.VMEM((4, 2, T, QUARTER // 2), BF16),
+            pltpu.VMEM((2, 2, ROWS, QUARTER), BF16),
+            pltpu.VMEM((4, 2, ROWS, QUARTER // 2), BF16),
             pltpu.VMEM((2, 2, 2, ROWS, QUARTER), BF16),
-            pltpu.VMEM((2, 2, 2, 2, ROWS, QUARTER), BF16),
+            pltpu.VMEM((4, 2, 2, ROWS, QUARTER // 2), BF16),
             pltpu.VMEM((T, D), BF16),
             pltpu.VMEM((F, T), BF16),
             pltpu.VMEM((ROWS, D), F32),
-            dma((4,)), dma((4,)), dma((2,)), dma((2, 12)), dma((3,)), dma((3, 4)), dma((10,)),
+            dma((4,)), dma((4,)), dma((2,)), dma((2, 14)), dma((3,)), dma((15,)), dma((10,)),
         ],
         compiler_params=pltpu.CompilerParams(
             collective_id=0, has_side_effects=True, vmem_limit_bytes=66000000

time: 68.6 us -> 67.5 us (0.984)
  Pallas kernels: 66.8 us -> 65.7 us
    pallas_call x1, Pallas kernels: 66.8 us -> 65.7 us  [layer(): pl.pallas_call(layer_kernel, out_shape=jax.ShapeDtypeStruct((ROWS, D), BF...]
where the time goes in v5:
time: 67.5 us; the launch traced here: 67.4 us
  Pallas kernels  65.7 us (97%)
  local copies, waits for them, and re-layouts  1.67 us (2%)
    pallas_call x1, Pallas kernels, layer(): pl.pallas_call(layer_kernel, out_shape=jax.ShapeDtypeStruct((ROWS, D), BF...  65.7 us
    unnamed x1, local copies, waits for them, and re-layouts  1.67 us

profile of v5, /device:TPU:1, one launch (start us, length us, event | category | flops | bytes accessed | tf_op | source)
XLA Modules:
  0.0 67.4 jit_solution(2982850425599243072)
XLA Ops:
  0.0 65.7 %layer.1 = bf16[64,2048]{1,0:T(8,128)(2,1)} custom-call(bf16[256,512]{1,0:T(8,128)(2,1)} %u_hbm.1, f32[32,256]{1,0:T(8,128)} %bitcast.17, f32[32,64]{1,0:T(8,128)} %pr_hbm.1, f32[32,64]{1,0:T(8,128)} %pi_hbm.1, f32[1,32]{1,0:T(1,128)} %bitcast.21, f32[512,64]{1,0:T(8,128)} %bitcast.13, f32[512,64]{1,0:T(8,128)} %bitcast.14, f32[512,64]{1,0:T(8,128)} %bitcast.15, ...), custom_call_target="tpu_custom_call" | custom-call | tf_op jit(solution)/shard_map/layer/pallas_call | solution.py:587
  65.7 1.7 %copy.19 = bf16[64,2048]{1,0:T(8,128)(2,1)} copy(bf16[64,2048]{1,0:T(8,128)(2,1)} %layer.1) | data formatting | bytes 524288

commit v6 on v5

--- a/solution.py
+++ b/solution.py
@@ -586,7 +586,7 @@
     dma = pltpu.SemaphoreType.DMA
     return pl.pallas_call(
         layer_kernel,
-        out_shape=jax.ShapeDtypeStruct((ROWS, D), BF16),
+        out_shape=pltpu.VMEM((ROWS, D), BF16),
         in_specs=[hbm] * len(arrays),
         out_specs=pl.BlockSpec(memory_space=pltpu.VMEM),
         scratch_shapes=[
@@ -621,7 +621,7 @@
             dma((4,)), dma((4,)), dma((2,)), dma((2, 14)), dma((3,)), dma((15,)), dma((10,)),
         ],
         compiler_params=pltpu.CompilerParams(
-            collective_id=0, has_side_effects=True, vmem_limit_bytes=66000000
+            collective_id=0, has_side_effects=True, vmem_limit_bytes=60000000
         ),
         name="layer",
     )(*arrays)

time: 67.5 us -> 65.8 us (0.975)
  local copies, waits for them, and re-layouts: 1.67 us -> 0.71 us
  Pallas kernels: 65.7 us -> 65 us
    unnamed x1, local copies, waits for them, and re-layouts: 1.67 us -> 0.71 us
    pallas_call x1, Pallas kernels: 65.7 us -> 65 us  [layer(): pl.pallas_call(layer_kernel, out_shape=pltpu.VMEM((ROWS, D), BF16), in_sp...]
where the time goes in v6:
time: 65.8 us; the launch traced here: 65.7 us
  Pallas kernels  65 us (99%)
  local copies, waits for them, and re-layouts  0.71 us (1%)
    pallas_call x1, Pallas kernels, layer(): pl.pallas_call(layer_kernel, out_shape=pltpu.VMEM((ROWS, D), BF16), in_sp...  65 us

profile of v6, /device:TPU:1, one launch (start us, length us, event | category | flops | bytes accessed | tf_op | source)
XLA Modules:
  0.0 65.7 jit_solution(13322735589448080544)
XLA Ops:
  0.0 65.0 %layer.1 = bf16[64,2048]{1,0:T(8,128)(2,1)S(1)} custom-call(bf16[256,512]{1,0:T(8,128)(2,1)} %u_hbm.1, f32[32,256]{1,0:T(8,128)} %bitcast.17, f32[32,64]{1,0:T(8,128)} %pr_hbm.1, f32[32,64]{1,0:T(8,128)} %pi_hbm.1, f32[1,32]{1,0:T(1,128)} %bitcast.21, f32[512,64]{1,0:T(8,128)} %bitcast.13, f32[512,64]{1,0:T(8,128)} %bitcast.14, f32[512,64]{1,0:T(8,128)} %bitcast.15, ...), custom_call_target="tpu_custom_call" | custom-call | tf_op jit(solution)/shard_map/layer/pallas_call | solution.py:587
  65.0 0.7 %copy.19 = bf16[64,2048]{1,0:T(8,128)(2,1)} copy(bf16[64,2048]{1,0:T(8,128)(2,1)S(1)} %layer.1) | data formatting | bytes 524288

commit v7 on v6

--- a/solution.py
+++ b/solution.py
@@ -229,15 +229,24 @@
         self.beyond_s(0, 0)
 
     def along_s(self, p, k):
-        ref = self.block(p, k, 0)
-        self.send(p, 3 + k, ref, self.s_next)
-        self.send(p, 3 + k, ref, self.s_prev)
+        if (p, k) == (1, 3):
+            top, bottom = self.block(p, k, 0, 0), self.block(p, k, 0, 1)
+            self.send(p, 6, top, self.s_next)
+            self.send(p, 6, bottom, self.s_prev)
+            self.send(p, 14, bottom, self.s_next)
+            self.send(p, 14, top, self.s_prev)
+        else:
+            ref = self.block(p, k, 0)
+            self.send(p, 3 + k, ref, self.s_next)
+            self.send(p, 3 + k, ref, self.s_prev)
         self.hand(p, k, 0)
 
     def beyond_s(self, p, k):
-        self.arrive(p, 3 + k, 128)
+        self.arrive(p, 3 + k, 64 if (p, k) == (1, 3) else 128)
         self.send(p, 7 + k, self.block(p, k, 1, 0), self.s_next)
         self.send(p, 7 + k, self.block(p, k, 2, 1), self.s_prev)
+        if (p, k) == (1, 3):
+            self.arrive(p, 14, 64)
         self.hand(p, k, 1)
         self.hand(p, k, 2)
 
@@ -539,8 +548,8 @@
     for first in range(0, F - 128, 256):
         tile = [gu_ref[:, side * F + first : side * F + first + 256] for side in range(2)]
         hidden_tile(dot(rows_ref[...], tile[0]), dot(rows_ref[...], tile[1]), first)
-        if first in (256, 1024):
-            weights.beyond_s(1, 1 if first == 256 else 2)
+        if first in (0, 768):
+            weights.beyond_s(1, 1 if first == 0 else 2)
     both = dot(rows_ref[...], jnp.concatenate([gu_ref[:, F - 128 : F], gu_ref[:, 2 * F - 128 :]], axis=1))
     hidden_tile(both[:, :128], both[:, 128:], F - 128)
 
@@ -618,7 +627,7 @@
             pltpu.VMEM((T, D), BF16),
             pltpu.VMEM((F, T), BF16),
             pltpu.VMEM((ROWS, D), F32),
-            dma((4,)), dma((4,)), dma((2,)), dma((2, 14)), dma((3,)), dma((15,)), dma((10,)),
+            dma((4,)), dma((4,)), dma((2,)), dma((2, 15)), dma((3,)), dma((15,)), dma((10,)),
         ],
         compiler_params=pltpu.CompilerParams(
             collective_id=0, has_side_effects=True, vmem_limit_bytes=60000000

time: 65.8 us -> 66 us (level)
  no operation moved by 1% of the time
where the time goes in v7:
time: 66 us; the launch traced here: 65.9 us
  Pallas kernels  65.2 us (99%)
  local copies, waits for them, and re-layouts  0.71 us (1%)
    pallas_call x1, Pallas kernels, layer(): pl.pallas_call(layer_kernel, out_shape=pltpu.VMEM((ROWS, D), BF16), in_sp...  65.2 us

profile of v7, /device:TPU:1, one launch (start us, length us, event | category | flops | bytes accessed | tf_op | source)
XLA Modules:
  0.0 65.9 jit_solution(9226582993216573443)
XLA Ops:
  0.0 65.2 %layer.1 = bf16[64,2048]{1,0:T(8,128)(2,1)S(1)} custom-call(bf16[256,512]{1,0:T(8,128)(2,1)} %u_hbm.1, f32[32,256]{1,0:T(8,128)} %bitcast.17, f32[32,64]{1,0:T(8,128)} %pr_hbm.1, f32[32,64]{1,0:T(8,128)} %pi_hbm.1, f32[1,32]{1,0:T(1,128)} %bitcast.21, f32[512,64]{1,0:T(8,128)} %bitcast.13, f32[512,64]{1,0:T(8,128)} %bitcast.14, f32[512,64]{1,0:T(8,128)} %bitcast.15, ...), custom_call_target="tpu_custom_call" | custom-call | tf_op jit(solution)/shard_map/layer/pallas_call | solution.py:596
  65.2 0.7 %copy.19 = bf16[64,2048]{1,0:T(8,128)(2,1)} copy(bf16[64,2048]{1,0:T(8,128)(2,1)S(1)} %layer.1) | data formatting | bytes 524288

commit v8 on v6

--- a/solution.py
+++ b/solution.py
@@ -273,9 +273,9 @@
             return pl.ds(pl.multiple_of(x * ROWS, ROWS), ROWS)
         return pl.ds(pl.multiple_of(x * ROWS + half * 32, 32), 32)
 
-    def start_relay(self, phase, g, part, relay):
-        self.send(phase, g, part.at[g, 0, self.rows(self.far)], relay.at[g, 0], self.next)
-        self.send(phase, g, part.at[g, 1, self.rows(self.far)], relay.at[g, 1], self.prev)
+    def start_relay(self, phase, g, side, part, relay):
+        dev = (self.next, self.prev)[side]
+        self.send(phase, g, part.at[g, side, self.rows(self.far)], relay.at[g, side], dev)
 
     def start_own(self, phase, g, part, landed):
         self.send(
@@ -501,7 +501,8 @@
         out = dot(act, wo_ref[:, g * HALF : (g + 1) * HALF]).astype(BF16)
         mix_part[g, 0] = out[:, :QUARTER]
         mix_part[g, 1] = out[:, QUARTER:]
-        across.start_relay(0, g, mix_part, mix_relay)
+        for side in range(2):
+            across.start_relay(0, g, side, mix_part, mix_relay)
         across.start_own(0, g, mix_part, mix_landed)
     weights.beyond_s_own()
     across.pass_on(0, 0, mix_part, mix_relay, mix_landed)
@@ -546,13 +547,17 @@
 
     def down(g):
         weights.handed_group(g)
-        block = jnp.concatenate(
-            [dn_ref[pl.ds(weights.columns(k, m), 128), :] for k, m in CHIPS[g]], axis=0)
-        out = dot(block, hid_ref[...])
-        for i in range(4):
-            out_part[g, i // 2, :, (i % 2) * 128 : (i % 2 + 1) * 128] = (
-                out[i * 128 : (i + 1) * 128].T.astype(BF16))
-        across.start_relay(1, g, out_part, out_relay)
+        size = 2 if g == 3 else 4
+        for start in range(0, 4, size):
+            block = jnp.concatenate(
+                [dn_ref[pl.ds(weights.columns(k, m), 128), :]
+                 for k, m in CHIPS[g][start : start + size]], axis=0)
+            out = dot(block, hid_ref[...])
+            for i in range(start, start + size):
+                out_part[g, i // 2, :, (i % 2) * 128 : (i % 2 + 1) * 128] = (
+                    out[(i - start) * 128 : (i - start + 1) * 128].T.astype(BF16))
+            for side in range(start // 2, (start + size) // 2):
+                across.start_relay(1, g, side, out_part, out_relay)
         across.start_own(1, g, out_part, out_landed)
 
     down(0)

time: 65.8 us -> 65.7 us (level)
  no operation moved by 1% of the time
where the time goes in v8:
time: 65.7 us
  Pallas kernels  64.9 us (99%)
  local copies, waits for them, and re-layouts  0.71 us (1%)
    pallas_call x1, Pallas kernels, layer(): pl.pallas_call(layer_kernel, out_shape=pltpu.VMEM((ROWS, D), BF16), in_sp...  64.9 us

profile of v8, /device:TPU:1, one launch (start us, length us, event | category | flops | bytes accessed | tf_op | source)
XLA Modules:
  0.0 65.7 jit_solution(2516887683476721582)
XLA Ops:
  0.0 64.9 %layer.1 = bf16[64,2048]{1,0:T(8,128)(2,1)S(1)} custom-call(bf16[256,512]{1,0:T(8,128)(2,1)} %u_hbm.1, f32[32,256]{1,0:T(8,128)} %bitcast.17, f32[32,64]{1,0:T(8,128)} %pr_hbm.1, f32[32,64]{1,0:T(8,128)} %pi_hbm.1, f32[1,32]{1,0:T(1,128)} %bitcast.21, f32[512,64]{1,0:T(8,128)} %bitcast.13, f32[512,64]{1,0:T(8,128)} %bitcast.14, f32[512,64]{1,0:T(8,128)} %bitcast.15, ...), custom_call_target="tpu_custom_call" | custom-call | tf_op jit(solution)/shard_map/layer/pallas_call | solution.py:592
  64.9 0.7 %copy.19 = bf16[64,2048]{1,0:T(8,128)(2,1)} copy(bf16[64,2048]{1,0:T(8,128)(2,1)S(1)} %layer.1) | data formatting | bytes 524288
